TPU v7x, 32 devices: a whole 2x2x4 slice. The times are simulated.
32 devices in a mesh: sp: 8 (over z, x), tp: 4 (over y, core).
Axes of the slice: x: 2, y: 2, z: 4, core: 2. Of those that a mesh axis runs over, the one named last changes fastest.
Arguments:
- queries: bfloat16 [1024, 2048], P('sp', 'tp'), may hold values from -440 to 440
- key_rows: bfloat16 [1024, 1024], P('sp', 'tp'), may hold values from -6 to 6
- value_rows: bfloat16 [1024, 1024], P('sp', 'tp'), may hold values from -6 to 6
- sink_logits: float32 [32], P('tp'), may hold values from -6 to 6
- out_weight: bfloat16 [2048, 2048], P('tp'), may hold values from -0.125 to 0.125
- residual: bfloat16 [1024, 2048], P('sp'), may hold values from -3 to 3
- norm_gain: float32 [2048], replicated, may hold values from 0.1 to 1.9
- routes: int32 [1024, 2], P('sp'), may hold values from 0 to 7, all different within a row; in each aligned block of 128 rows (0 to 127, 128 to 255, ...) at most 64 rows name the same one
- route_weights: float32 [1024, 2], P('sp'), may hold values from 0.2 to 1
- gate_weight: bfloat16 [8, 2048, 4096], P('sp', None, 'tp'), may hold values from -0.125 to 0.125
- up_weight: bfloat16 [8, 2048, 4096], P('sp', None, 'tp'), may hold values from -0.125 to 0.125
- down_weight: bfloat16 [8, 4096, 2048], P('sp', 'tp'), may hold values from -0.09375 to 0.09375
Outputs:
- layer_out: bfloat16 [1024, 2048], P('sp')
Inputs may be any that keep to these rules, and one draw needn't show every extreme that they name: `routes`: each row names 2 different experts. In each aligned block of 128 rows (the rows of one index of sp) no expert is named by more than 64 rows, a bound that some block reaches.
All inputs are finite; a program needn't handle non-finite values.
Results may differ from a plain program's by a relative error of at most 0.02.
Values may be sent and summed in bfloat16 or wider, within the bound.
A program may use at most 64 MiB of HBM per device.

v0:
```python
import functools

import jax
import jax.numpy as jnp
import numpy as np
from jax import lax
from jax.experimental import pallas as pl
from jax.experimental.pallas import tpu as pltpu
from jax.sharding import PartitionSpec as P

HEAD_DIM = 64
WINDOW = 128
TOP = 2
CORES = 2
F32 = jnp.float32
BF16 = jnp.bfloat16
MESH = pl.DeviceIdType.MESH


def kernel(
    S,
    T,
    slope_ref,
    sink_ref,
    q_ref,
    k_ref,
    v_ref,
    res_ref,
    gain_ref,
    routes_ref,
    rw_ref,
    wo_hbm,
    wg_hbm,
    wu_hbm,
    wd_hbm,
    out_ref,
    wo,
    wg,
    wu,
    wd,
    halo,
    att,
    pp,
    rc1,
    sb1,
    ry1,
    mixed,
    picked,
    x_all,
    xn,
    act,
    yp,
    rc2,
    sb2,
    ry2,
    rb,
    ret,
    o_all,
    w_sem,
    halo_s,
    halo_r,
    c1_s,
    c1_r,
    y1_s,
    y1_r,
    a_s,
    a_r,
    fy_s,
    fy_r,
    fc_s,
    fc_r,
    c2_s,
    c2_r,
    y2_s,
    y2_r,
    b_s,
    b_r,
    gy_s,
    gy_r,
    gc_s,
    gc_r,
):
    R, D = res_ref.shape
    Y = T // CORES
    W = D // T
    H = q_ref.shape[1] // HEAD_DIM
    KV = k_ref.shape[1] // HEAD_DIM
    G = H // KV
    C = x_all.shape[0] // S
    half = S // 2
    GM = half * C
    FL = wg.shape[1]

    me = lax.axis_index("sp")
    t = lax.axis_index("tp")
    y = t // CORES
    c = t % CORES
    oc = 1 - c

    def tp_of(yy, cc):
        return yy * CORES + cc

    def cols(tt):
        return pl.ds(pl.multiple_of(tt * W, W), W)

    def rows(s):
        return pl.ds(pl.multiple_of(s * C, C), C)

    def yo(d):
        return (y + d) % Y

    def remote(src, dst, ss, rs, **dev):
        return pltpu.make_async_remote_copy(
            src_ref=src, dst_ref=dst, send_sem=ss, recv_sem=rs, device_id=dev, device_id_type=MESH
        )

    loads = [
        pltpu.make_async_copy(wo_hbm, wo, w_sem.at[0]),
        pltpu.make_async_copy(wg_hbm.at[0], wg, w_sem.at[1]),
        pltpu.make_async_copy(wu_hbm.at[0], wu, w_sem.at[2]),
        pltpu.make_async_copy(wd_hbm.at[0], wd, w_sem.at[3]),
    ]
    for load in loads:
        load.start()

    barrier = pltpu.get_barrier_semaphore()

    @pl.loop(1, S)
    def _(d):
        pl.semaphore_signal(
            barrier, inc=1, device_id={"sp": (me + d) % S}, device_id_type=MESH
        )

    for d in range(1, Y):
        pl.semaphore_signal(
            barrier, inc=1, device_id={"tp": tp_of(yo(d), c)}, device_id_type=MESH
        )
    pl.semaphore_signal(barrier, inc=1, device_id={"tp": tp_of(y, oc)}, device_id_type=MESH)
    pl.semaphore_wait(barrier, S - 1 + Y)

    halo_copies = [
        remote(src, halo.at[i], halo_s.at[i], halo_r.at[i], sp=jnp.minimum(me + 1, S - 1))
        for i, src in enumerate((k_ref, v_ref))
    ]

    @pl.when(me < S - 1)
    def _():
        for copy in halo_copies:
            copy.start()

    def column(row):
        return jnp.broadcast_to(row, (R, R)).T[:, 0:1]

    r0 = column(routes_ref[0:1, :].astype(F32)).astype(jnp.int32)
    r1 = column(routes_ref[1:2, :].astype(F32)).astype(jnp.int32)
    lane_e = lax.broadcasted_iota(jnp.int32, (R, 128), 1)
    hit0 = lane_e == r0
    hit1 = lane_e == r1
    member = jnp.where(hit0 | hit1, 1.0, 0.0).astype(BF16)
    tri = jnp.where(
        lax.broadcasted_iota(jnp.int32, (R, R), 1) < lax.broadcasted_iota(jnp.int32, (R, R), 0),
        1.0,
        0.0,
    ).astype(BF16)
    rank = jnp.dot(tri, member, preferred_element_type=F32)
    rank0 = jnp.sum(jnp.where(hit0, rank, 0.0), axis=1, keepdims=True)
    rank1 = jnp.sum(jnp.where(hit1, rank, 0.0), axis=1, keepdims=True)
    slot0 = r0.astype(F32) * C + rank0
    slot1 = r1.astype(F32) * C + rank1
    lane_s = lax.broadcasted_iota(jnp.int32, (R, S * C), 1).astype(F32)

    def picker(slot):
        return jnp.where(lane_s == slot, 1.0, 0.0)

    qi = lax.broadcasted_iota(jnp.int32, (R, R), 0)
    kj = lax.broadcasted_iota(jnp.int32, (R, R), 1)
    dist_own = (qi - kj).astype(F32)
    dist_old = (qi - kj + WINDOW).astype(F32)
    nt = (((1,), (1,)), ((), ()))

    ok_own = qi >= kj
    ok_old = (kj >= qi) & (kj + me * R >= WINDOW)

    def head(h):
        return slice(h * HEAD_DIM, (h + 1) * HEAD_DIM), slice(
            (h // G) * HEAD_DIM, (h // G + 1) * HEAD_DIM
        )

    def scores(h, keys, dist, ok):
        raw = lax.dot_general(q_ref[:, head(h)[0]], keys, nt, preferred_element_type=F32)
        return jnp.where(ok, raw * HEAD_DIM**-0.5 - slope_ref[t * H + h] * dist, -jnp.inf)

    own = [scores(h, k_ref[:, head(h)[1]], dist_own, ok_own) for h in range(H)]
    own_peak = [jnp.max(x, axis=1, keepdims=True) for x in own]

    @pl.when(me > 0)
    def _():
        for copy in halo_copies:
            copy.wait_recv()

    @pl.when(me == 0)
    def _():
        halo[...] = jnp.zeros_like(halo)

    for h in range(H):
        hc, kc = head(h)
        s_own = own[h]
        s_old = scores(h, halo[0, :, kc], dist_old, ok_old)
        peak = jnp.maximum(own_peak[h], jnp.max(s_old, axis=1, keepdims=True))
        e_own = jnp.exp(s_own - peak)
        e_old = jnp.exp(s_old - peak)
        total = jnp.sum(e_own, axis=1, keepdims=True) + jnp.sum(e_old, axis=1, keepdims=True)
        inv = 1.0 / total
        mix = jnp.dot((e_own * inv).astype(BF16), v_ref[:, kc], preferred_element_type=F32)
        mix += jnp.dot((e_old * inv).astype(BF16), halo[1, :, kc], preferred_element_type=F32)
        keep = 1.0 / (1.0 + jnp.exp(sink_ref[h] - peak - jnp.log(total)))
        att[:, hc] = (mix * keep).astype(BF16)

    loads[0].wait()

    def project(tt):
        pp[:, cols(tt)] = jnp.dot(att[...], wo[:, cols(tt)], preferred_element_type=F32).astype(
            BF16
        )

    def c1(yy):
        return remote(
            pp.at[:, cols(tp_of(yy, oc))], rc1.at[yy], c1_s.at[yy], c1_r.at[yy], tp=tp_of(y, oc)
        )

    def y1_send(yy):
        return remote(sb1.at[yy], ry1.at[y], y1_s.at[yy], y1_r.at[y], tp=tp_of(yy, c))

    def y1_recv(yy):
        return remote(sb1.at[yy], ry1.at[yy], y1_s.at[yy], y1_r.at[yy], tp=tp_of(yy, c))

    for d in list(range(1, Y)) + [0]:
        project(tp_of(yo(d), oc))
        c1(yo(d)).start()
    for d in list(range(1, Y)) + [0]:
        project(tp_of(yo(d), c))
    for d in range(1, Y):
        c1(yo(d)).wait_recv()
        sb1[yo(d)] = (pp[:, cols(tp_of(yo(d), c))].astype(F32) + rc1[yo(d)].astype(F32)).astype(
            BF16
        )
        y1_send(yo(d)).start()
    c1(y).wait_recv()
    head_sum = pp[:, cols(t)].astype(F32) + rc1[y].astype(F32)
    for d in range(1, Y):
        y1_recv(yo(d)).wait_recv()
        head_sum = head_sum + ry1[yo(d)].astype(F32)
    mixed[...] = (res_ref[:, cols(t)].astype(F32) + head_sum).astype(BF16)

    both = (picker(slot0) + picker(slot1)).T.astype(BF16)
    picked[...] = jnp.dot(both, mixed[...], preferred_element_type=F32).astype(BF16)

    loc = me // 2
    near = me % 2
    far = 1 - near

    def source(par, p):
        return 2 * p + par

    def place(par, d):
        return source(par, (loc + half - d) % half)

    def spot(s):
        return rows((s % 2) * half + s // 2)

    def a_send(e):
        return remote(
            picked.at[rows(e)], x_all.at[spot(me), cols(t)], a_s.at[e], a_r.at[me], sp=e
        )

    def a_recv(s):
        return remote(picked.at[rows(s)], x_all.at[spot(s), cols(t)], a_s.at[s], a_r.at[s], sp=s)

    def fy_send(s, yy):
        ref = x_all.at[spot(s), cols(t)]
        return remote(ref, ref, fy_s.at[s, yy], fy_r.at[s, y], tp=tp_of(yy, c))

    def fy_recv(s, yy):
        ref = x_all.at[spot(s), cols(tp_of(yy, c))]
        return remote(ref, ref, fy_s.at[s, yy], fy_r.at[s, yy], tp=tp_of(yy, c))

    def fc_send(s, yy):
        ref = x_all.at[spot(s), cols(tp_of(yy, c))]
        return remote(ref, ref, fc_s.at[s, yy], fc_r.at[s, yy], tp=tp_of(y, oc))

    def fc_recv(s, yy):
        ref = x_all.at[spot(s), cols(tp_of(yy, oc))]
        return remote(ref, ref, fc_s.at[s, yy], fc_r.at[s, yy], tp=tp_of(y, oc))

    @pl.loop(1, half)
    def _(d):
        a_send(source(near, (loc + d) % half)).start()

    @pl.loop(0, half)
    def _(d):
        a_send(source(far, (loc + d) % half)).start()

    x_all[spot(me), cols(t)] = picked[rows(me)]

    def forward(s):
        for d in range(1, Y):
            fy_send(s, yo(d)).start()
        fc_send(s, y).start()

    def relay(s):
        for i in range(1, Y):
            fy_recv(s, yo(i)).wait_recv()
            fc_send(s, yo(i)).start()

    def arrive(s):
        a_recv(s).wait_recv()
        forward(s)

    def norm_group(base):
        @pl.loop(0, half)
        def _(d):
            s = place(base, d)
            for i in range(Y):
                fc_recv(s, yo(i)).wait_recv()
            x = x_all[spot(s)].astype(F32)
            scale = lax.rsqrt(jnp.mean(x * x, axis=1, keepdims=True) + 1e-06)
            xn[spot(s)] = (x * scale * gain_ref[...]).astype(BF16)

    TN = min(256, FL)

    def hidden_group(base):
        at = pl.ds(pl.multiple_of(base * GM, GM), GM)

        @pl.loop(0, FL // TN)
        def _(n):
            nn = pl.ds(pl.multiple_of(n * TN, TN), TN)
            gate = jnp.dot(xn[at], wg[:, nn], preferred_element_type=F32)
            up = jnp.dot(xn[at], wu[:, nn], preferred_element_type=F32)
            act[:, nn] = (gate / (1.0 + jnp.exp(-gate)) * up).astype(BF16)

    def c2(g, yy):
        return remote(
            yp.at[g, :, cols(tp_of(yy, oc))],
            rc2.at[g, yy],
            c2_s.at[g, yy],
            c2_r.at[g, yy],
            tp=tp_of(y, oc),
        )

    def down_block(g, tt):
        yp[g, :, cols(tt)] = jnp.dot(act[...], wd[:, cols(tt)], preferred_element_type=F32).astype(
            BF16
        )

    def down_group(g):
        @pl.loop(0, Y)
        def _(d):
            yy = yo(d + 1)
            down_block(g, tp_of(yy, oc))
            c2(g, yy).start()

        @pl.loop(0, Y)
        def _(d):
            down_block(g, tp_of(yo(d + 1), c))

    def y2_send(g, p, yy):
        return remote(
            sb2.at[g, yy, rows(p)],
            ry2.at[g, y, rows(p)],
            y2_s.at[g, p, yy],
            y2_r.at[g, p, y],
            tp=tp_of(yy, c),
        )

    def y2_recv(g, p, yy):
        return remote(
            sb2.at[g, yy, rows(p)],
            ry2.at[g, yy, rows(p)],
            y2_s.at[g, p, yy],
            y2_r.at[g, p, yy],
            tp=tp_of(yy, c),
        )

    def b_send(s):
        return remote(rb.at[rows(s)], ret.at[rows(me)], b_s.at[s], b_r.at[me], sp=s)

    def b_recv(s):
        return remote(rb.at[rows(s)], ret.at[rows(s)], b_s.at[s], b_r.at[s], sp=s)

    def pair_sum(g):
        for d in list(range(1, Y)) + [0]:
            yy = yo(d)
            c2(g, yy).wait_recv()

            @pl.loop(0, half)
            def _(i):
                p = (loc + half - i) % half
                sb2[g, yy, rows(p)] = (
                    yp[g, rows(p), cols(tp_of(yy, c))].astype(F32) + rc2[g, yy, rows(p)].astype(F32)
                ).astype(BF16)
                if d:
                    y2_send(g, p, yy).start()

    def send_back(g, base):
        @pl.loop(0, half)
        def _(i):
            p = (loc + half - i) % half
            s = source(base, p)
            total = sb2[g, y, rows(p)].astype(F32)
            for d in range(1, Y):
                y2_recv(g, p, yo(d)).wait_recv()
                total = total + ry2[g, yo(d), rows(p)].astype(F32)
            rb[rows(s)] = total.astype(BF16)

            @pl.when(s != me)
            def _():
                b_send(s).start()

    forward(me)

    @pl.loop(1, half)
    def _(d):
        arrive(place(near, d))

    @pl.loop(0, half)
    def _(d):
        relay(place(near, d))
        arrive(place(far, d))

    norm_group(near)
    loads[1].wait()
    loads[2].wait()
    hidden_group(near)

    loads[3].wait()
    down_group(0)

    @pl.loop(0, half)
    def _(d):
        relay(place(far, d))

    pair_sum(0)
    norm_group(far)
    hidden_group(far)
    send_back(0, near)
    down_group(1)
    pair_sum(1)
    send_back(1, far)

    ret[rows(me)] = rb[rows(me)]

    @pl.loop(1, S)
    def _(d):
        b_recv((me + d) % S).wait_recv()

    mix0 = jnp.dot(picker(slot0).astype(BF16), ret[...], preferred_element_type=F32)
    mix1 = jnp.dot(picker(slot1).astype(BF16), ret[...], preferred_element_type=F32)
    o_all[:, cols(t)] = (
        mixed[...].astype(F32) + (column(rw_ref[0:1, :]) * mix0 + column(rw_ref[1:2, :]) * mix1)
    ).astype(BF16)

    def gy_send(yy):
        ref = o_all.at[:, cols(t)]
        return remote(ref, ref, gy_s.at[yy], gy_r.at[y], tp=tp_of(yy, c))

    def gy_recv(yy):
        ref = o_all.at[:, cols(tp_of(yy, c))]
        return remote(ref, ref, gy_s.at[yy], gy_r.at[yy], tp=tp_of(yy, c))

    def gc_send(yy):
        ref = o_all.at[:, cols(tp_of(yy, c))]
        return remote(ref, ref, gc_s.at[yy], gc_r.at[yy], tp=tp_of(y, oc))

    def gc_recv(yy):
        ref = o_all.at[:, cols(tp_of(yy, oc))]
        return remote(ref, ref, gc_s.at[yy], gc_r.at[yy], tp=tp_of(y, oc))

    for d in range(1, Y):
        gy_send(yo(d)).start()
    gc_send(y).start()
    for d in range(1, Y):
        gy_recv(yo(d)).wait_recv()
        gc_send(yo(d)).start()
    for d in range(Y):
        gc_recv(yo(d)).wait_recv()
    out_ref[...] = o_all[...]

    @pl.when(me < S - 1)
    def _():
        for copy in halo_copies:
            copy.wait_send()

    for d in range(Y):
        c1(yo(d)).wait_send()
        gc_send(yo(d)).wait_send()
        for g in range(2):
            c2(g, yo(d)).wait_send()
    for d in range(1, Y):
        y1_send(yo(d)).wait_send()
        gy_send(yo(d)).wait_send()

    @pl.loop(1, S)
    def _(d):
        a_send((me + d) % S).wait_send()
        b_send((me + d) % S).wait_send()

    @pl.loop(0, S)
    def _(s):
        for d in range(Y):
            fc_send(s, yo(d)).wait_send()
        for d in range(1, Y):
            fy_send(s, yo(d)).wait_send()

    @pl.loop(0, half)
    def _(p):
        for d in range(1, Y):
            for g in range(2):
                y2_send(g, p, yo(d)).wait_send()


def per_device(
    S,
    T,
    queries,
    key_rows,
    value_rows,
    sink_logits,
    out_weight,
    residual,
    norm_gain,
    routes,
    route_weights,
    gate_weight,
    up_weight,
    down_weight,
):
    R, D = residual.shape
    HW = queries.shape[1]
    heads = HW // HEAD_DIM * T
    Y = T // CORES
    W = D // T
    C = 2 * R * TOP // S
    half = S // 2
    GM = half * C
    FL = gate_weight.shape[2]
    slopes = jnp.asarray(np.exp2(-8.0 * np.arange(1, heads + 1) / heads).astype(np.float32))
    vmem = pl.BlockSpec(memory_space=pltpu.VMEM)
    smem = pl.BlockSpec(memory_space=pltpu.SMEM)
    hbm = pl.BlockSpec(memory_space=pl.ANY)
    dma = pltpu.SemaphoreType.DMA
    v = pltpu.VMEM
    return pl.pallas_call(
        functools.partial(kernel, S, T),
        out_shape=jax.ShapeDtypeStruct((R, D), BF16),
        in_specs=[smem, smem] + [vmem] * 7 + [hbm] * 4,
        out_specs=vmem,
        scratch_shapes=[
            v(out_weight.shape, BF16),
            v(gate_weight.shape[1:], BF16),
            v(up_weight.shape[1:], BF16),
            v(down_weight.shape[1:], BF16),
            v((2,) + key_rows.shape, BF16),
            v((R, HW), BF16),
            v((R, D), BF16),
            v((Y, R, W), BF16),
            v((Y, R, W), BF16),
            v((Y, R, W), BF16),
            v((R, W), BF16),
            v((S * C, W), BF16),
            v((S * C, D), BF16),
            v((S * C, D), BF16),
            v((GM, FL), BF16),
            v((2, GM, D), BF16),
            v((2, Y, GM, W), BF16),
            v((2, Y, GM, W), BF16),
            v((2, Y, GM, W), BF16),
            v((S * C, W), BF16),
            v((S * C, W), BF16),
            v((R, D), BF16),
            dma((4,)),
            dma((2,)),
            dma((2,)),
            dma((Y,)),
            dma((Y,)),
            dma((Y,)),
            dma((Y,)),
            dma((S,)),
            dma((S,)),
            dma((S, Y)),
            dma((S, Y)),
            dma((S, Y)),
            dma((S, Y)),
            dma((2, Y)),
            dma((2, Y)),
            dma((2, half, Y)),
            dma((2, half, Y)),
            dma((S,)),
            dma((S,)),
            dma((Y,)),
            dma((Y,)),
            dma((Y,)),
            dma((Y,)),
        ],
        compiler_params=pltpu.CompilerParams(
            collective_id=0, has_side_effects=True, vmem_limit_bytes=60 * 1024 * 1024
        ),
        name="layer",
    )(
        slopes,
        sink_logits,
        queries,
        key_rows,
        value_rows,
        residual,
        norm_gain.reshape(1, D),
        routes.T,
        route_weights.T,
        out_weight,
        gate_weight,
        up_weight,
        down_weight,
    )


def solution(mesh):
    placed = (
        P("sp", "tp"),
        P("sp", "tp"),
        P("sp", "tp"),
        P("tp"),
        P("tp", None),
        P("sp", None),
        P(),
        P("sp", None),
        P("sp", None),
        P("sp", None, "tp"),
        P("sp", None, "tp"),
        P("sp", "tp", None),
    )
    return jax.shard_map(
        functools.partial(per_device, mesh.shape["sp"], mesh.shape["tp"]),
        mesh=mesh,
        in_specs=placed,
        out_specs=P("sp", None),
        check_vma=False,
    )
```

profile of v0, /device:TPU:0, one launch (start us, length us, event | category | flops | bytes accessed | tf_op | source)
XLA Modules:
  0.0 70.1 jit_solution(13217109295726205745)
XLA Ops:
  0.0 68.3 %layer.1 = bf16[128,2048]{1,0:T(8,128)(2,1)} custom-call(f32[32]{0:T(128)} %constant.2.clone.slope_ref, f32[8]{0:T(128)} %sink_ref.1, bf16[128,512]{1,0:T(8,128)(2,1)} %q_ref.1, bf16[128,256]{1,0:T(8,128)(2,1)} %k_ref.1, bf16[128,256]{1,0:T(8,128)(2,1)} %v_ref.1, bf16[128,2048]{1,0:T(8,128)(2,1)} %res_ref.1, f32[1,2048]{1,0:T(1,128)} %bitcast.3, ...), custom_call_target="tpu_custom_call" | custom-call | tf_op jit(solution)/shard_map/layer/pallas_call | solution.py:552
  68.3 1.9 %copy.15 = bf16[128,2048]{1,0:T(8,128)(2,1)} copy(bf16[128,2048]{1,0:T(8,128)(2,1)} %layer.1) | data formatting | bytes 1048576
where the time goes:
time: 71.2 us; the launch traced here: 70.1 us
  Pallas kernels  68.3 us (96%)
  local copies, waits for them, and re-layouts  1.88 us (3%)
    pallas_call x1, Pallas kernels, per_device(): pl.pallas_call(functools.partial(kernel, S, T), out_shape=jax.ShapeDtypeS...  68.3 us
    unnamed x1, local copies, waits for them, and re-layouts  1.88 us

commit v1 on v0

v1 whole, which is shorter than its diff:
```python
import functools

import jax
import jax.numpy as jnp
import numpy as np
from jax import lax
from jax.experimental import pallas as pl
from jax.experimental.pallas import tpu as pltpu
from jax.sharding import PartitionSpec as P

HEAD_DIM = 64
WINDOW = 128
TOP = 2
CORES = 2
F32 = jnp.float32
BF16 = jnp.bfloat16
MESH = pl.DeviceIdType.MESH


def kernel(
    S,
    T,
    sink_hbm,
    q_hbm,
    k_hbm,
    v_hbm,
    res_hbm,
    gain_hbm,
    routes_hbm,
    rw_hbm,
    wo_hbm,
    wg_hbm,
    wu_hbm,
    wd_hbm,
    out_hbm,
    sink,
    q,
    k,
    v,
    res,
    gain,
    routes,
    rw,
    wo,
    wg,
    wu,
    wd,
    halo,
    att,
    pp,
    rc1,
    sb1,
    ry1,
    mixed,
    picked,
    x_all,
    xn,
    act,
    yp,
    rc2,
    sb2,
    ry2,
    rb,
    ret,
    o_all,
    w_sem,
    halo_s,
    halo_r,
    c1_s,
    c1_r,
    y1_s,
    y1_r,
    a_s,
    a_r,
    fy_s,
    fy_r,
    fc_s,
    fc_r,
    c2_s,
    c2_r,
    y2_s,
    y2_r,
    b_s,
    b_r,
    gy_s,
    gy_r,
    gc_s,
    gc_r,
    o_sem,
):
    R, W = res.shape
    D = W * T
    Y = T // CORES
    H = q.shape[1] // HEAD_DIM
    KV = k.shape[1] // HEAD_DIM
    G = H // KV
    C = x_all.shape[0] // S
    Z = S // 2
    NEAR = (Z + 1) * C
    FL = wg.shape[1]
    NH = y1_s.shape[1]
    HW = W // NH

    me = lax.axis_index("sp")
    t = lax.axis_index("tp")
    y = t // CORES
    c = t % CORES
    oc = 1 - c
    z = me // 2
    x = me % 2

    def tp_of(yy, cc):
        return yy * CORES + cc

    def cols(tt):
        return pl.ds(pl.multiple_of(tt * W, W), W)

    def part(tt, j):
        return pl.ds(pl.multiple_of(tt * W + j * HW, HW), HW)

    def rows(s):
        return pl.ds(pl.multiple_of(s * C, C), C)

    def yo(d):
        return (y + d) % Y

    def remote(src, dst, ss, rs, **dev):
        return pltpu.make_async_remote_copy(
            src_ref=src, dst_ref=dst, send_sem=ss, recv_sem=rs, device_id=dev, device_id_type=MESH
        )

    def peer(p):
        zz = z
        bit = 1
        while bit < Z:
            if (p % Z) // bit % 2:
                zz = zz + bit * (1 - 2 * (zz // bit % 2))
            bit *= 2
        return 2 * zz + (x + p // Z) % 2

    far = list(range(Z + 1, 2 * Z))
    near = list(range(Z + 1))
    groups = ((0, near), (NEAR, far))

    def span(p):
        return pl.ds(p * C, C)

    def local(p):
        return pl.ds((p if p <= Z else p - Z - 1) * C, C)

    def group(p):
        return 0 if p <= Z else 1

    barrier = pltpu.get_barrier_semaphore()

    @pl.loop(1, S)
    def _(d):
        pl.semaphore_signal(
            barrier, inc=1, device_id={"sp": (me + d) % S}, device_id_type=MESH
        )

    for d in range(1, Y):
        pl.semaphore_signal(
            barrier, inc=1, device_id={"tp": tp_of(yo(d), c)}, device_id_type=MESH
        )
    pl.semaphore_signal(barrier, inc=1, device_id={"tp": tp_of(y, oc)}, device_id_type=MESH)

    loads = [
        pltpu.make_async_copy(src, dst, w_sem.at[i])
        for i, (src, dst) in enumerate(
            (
                (k_hbm, k),
                (v_hbm, v),
                (q_hbm, q),
                (routes_hbm, routes),
                (sink_hbm, sink),
                (res_hbm.at[:, cols(t)], res),
                (rw_hbm, rw),
                (gain_hbm, gain),
                (wo_hbm, wo),
                (wg_hbm.at[0], wg),
                (wu_hbm.at[0], wu),
                (wd_hbm.at[0], wd),
            )
        )
    ]
    for load in loads:
        load.start()
    loads[0].wait()
    loads[1].wait()
    pl.semaphore_wait(barrier, S - 1 + Y)

    halo_copies = [
        remote(src, halo.at[i], halo_s.at[i], halo_r.at[i], sp=jnp.minimum(me + 1, S - 1))
        for i, src in enumerate((k, v))
    ]

    @pl.when(me < S - 1)
    def _():
        for copy in halo_copies:
            copy.start()

    for load in loads[2:5]:
        load.wait()

    qi = lax.broadcasted_iota(jnp.int32, (R, R), 0)
    kj = lax.broadcasted_iota(jnp.int32, (R, R), 1)
    dist_own = (qi - kj).astype(F32)
    dist_old = (qi - kj + WINDOW).astype(F32)
    nt = (((1,), (1,)), ((), ()))

    ok_own = qi >= kj
    ok_old = (kj >= qi) & (kj + me * R >= WINDOW)

    base = jnp.float32(1.0)
    for i in range(1, T):
        base = jnp.where(t == i, jnp.float32(2.0 ** (-8.0 * i / T)), base)

    def head(h):
        return slice(h * HEAD_DIM, (h + 1) * HEAD_DIM), slice(
            (h // G) * HEAD_DIM, (h // G + 1) * HEAD_DIM
        )

    def scores(h, keys, dist, ok):
        raw = lax.dot_general(q[:, head(h)[0]], keys, nt, preferred_element_type=F32)
        slope = base * np.float32(2.0 ** (-8.0 * (h + 1) / (H * T)))
        return jnp.where(ok, raw * HEAD_DIM**-0.5 - slope * dist, -jnp.inf)

    own = []
    for h in range(H):
        s_own = scores(h, k[:, head(h)[1]], dist_own, ok_own)
        top = jnp.max(s_own, axis=1, keepdims=True)
        e_own = jnp.exp(s_own - top)
        own.append(
            (
                top,
                jnp.sum(e_own, axis=1, keepdims=True),
                jnp.dot(e_own.astype(BF16), v[:, head(h)[1]], preferred_element_type=F32),
            )
        )

    def column(row):
        return jnp.broadcast_to(row, (R, R)).T[:, 0:1]

    r0 = column(routes[0:1, :].astype(F32)).astype(jnp.int32)
    r1 = column(routes[1:2, :].astype(F32)).astype(jnp.int32)
    lane_e = lax.broadcasted_iota(jnp.int32, (R, 128), 1)
    hit0 = lane_e == r0
    hit1 = lane_e == r1
    member = jnp.where(hit0 | hit1, 1.0, 0.0).astype(BF16)
    tri = jnp.where(
        lax.broadcasted_iota(jnp.int32, (R, R), 1) < lax.broadcasted_iota(jnp.int32, (R, R), 0),
        1.0,
        0.0,
    ).astype(BF16)
    rank = jnp.dot(tri, member, preferred_element_type=F32)
    rank0 = jnp.sum(jnp.where(hit0, rank, 0.0), axis=1, keepdims=True)
    rank1 = jnp.sum(jnp.where(hit1, rank, 0.0), axis=1, keepdims=True)
    slot0 = r0.astype(F32) * C + rank0
    slot1 = r1.astype(F32) * C + rank1
    lane_s = lax.broadcasted_iota(jnp.int32, (R, S * C), 1).astype(F32)

    def picker(slot):
        return jnp.where(lane_s == slot, 1.0, 0.0)

    both = (picker(slot0) + picker(slot1)).T.astype(BF16)

    @pl.when(me > 0)
    def _():
        for copy in halo_copies:
            copy.wait_recv()

    @pl.when(me == 0)
    def _():
        halo[...] = jnp.zeros_like(halo)

    for h in range(H):
        hc, kc = head(h)
        top, weight, mix = own[h]
        s_old = scores(h, halo[0, :, kc], dist_old, ok_old)
        peak = jnp.maximum(top, jnp.max(s_old, axis=1, keepdims=True))
        shrink = jnp.exp(top - peak)
        e_old = jnp.exp(s_old - peak)
        total = weight * shrink + jnp.sum(e_old, axis=1, keepdims=True)
        mix = mix * shrink + jnp.dot(
            e_old.astype(BF16), halo[1, :, kc], preferred_element_type=F32
        )
        keep = 1.0 / (total + jnp.exp(sink[0:1, h : h + 1] - peak))
        att[:, hc] = (mix * keep).astype(BF16)

    for load in loads[5:9]:
        load.wait()

    def project(tt):
        pp[:, cols(tt)] = jnp.dot(att[...], wo[:, cols(tt)], preferred_element_type=F32).astype(
            BF16
        )

    def c1(yy):
        return remote(
            pp.at[:, cols(tp_of(yy, oc))], rc1.at[yy], c1_s.at[yy], c1_r.at[yy], tp=tp_of(y, oc)
        )

    def y1_send(yy, j):
        return remote(
            sb1.at[yy, j], ry1.at[y, j], y1_s.at[yy, j], y1_r.at[y, j], tp=tp_of(yy, c)
        )

    def y1_recv(yy, j):
        return remote(
            sb1.at[yy, j], ry1.at[yy, j], y1_s.at[yy, j], y1_r.at[yy, j], tp=tp_of(yy, c)
        )

    turns = list(range(1, Y)) + [0]

    def half(j):
        return slice(j * HW, (j + 1) * HW)

    for d in turns:
        project(tp_of(yo(d), oc))
        c1(yo(d)).start()
    for d in turns:
        project(tp_of(yo(d), c))
    for d in range(1, Y):
        c1(yo(d)).wait_recv()
        for j in range(NH):
            sb1[yo(d), j] = (
                pp[:, part(tp_of(yo(d), c), j)].astype(F32) + rc1[yo(d), :, half(j)].astype(F32)
            ).astype(BF16)
            y1_send(yo(d), j).start()
    c1(y).wait_recv()

    def a_send(p, j):
        e = peer(p)
        return remote(
            picked.at[rows(e), half(j)],
            x_all.at[span(p), part(t, j)],
            a_s.at[p, j],
            a_r.at[p, j],
            sp=e,
        )

    def fy_send(p, yy):
        ref = x_all.at[span(p), cols(t)]
        return remote(ref, ref, fy_s.at[p, yy], fy_r.at[p, y], tp=tp_of(yy, c))

    def fy_recv(p, yy):
        ref = x_all.at[span(p), cols(tp_of(yy, c))]
        return remote(ref, ref, fy_s.at[p, yy], fy_r.at[p, yy], tp=tp_of(yy, c))

    def fc_send(p, yy):
        ref = x_all.at[span(p), cols(tp_of(yy, c))]
        return remote(ref, ref, fc_s.at[p, yy], fc_r.at[p, yy], tp=tp_of(y, oc))

    def fc_recv(p, yy):
        ref = x_all.at[span(p), cols(tp_of(yy, oc))]
        return remote(ref, ref, fc_s.at[p, yy], fc_r.at[p, yy], tp=tp_of(y, oc))

    outward = [Z] + list(range(1, Z)) + far

    for j in range(NH):
        head_sum = pp[:, part(t, j)].astype(F32) + rc1[y, :, half(j)].astype(F32)
        for d in range(1, Y):
            y1_recv(yo(d), j).wait_recv()
            head_sum = head_sum + ry1[yo(d), j].astype(F32)
        mixed[:, half(j)] = (res[:, half(j)].astype(F32) + head_sum).astype(BF16)
        picked[:, half(j)] = jnp.dot(
            both, mixed[:, half(j)], preferred_element_type=F32
        ).astype(BF16)
        for p in outward:
            a_send(p, j).start()
    x_all[span(0), cols(t)] = picked[rows(me)]

    def forward(p):
        for d in range(1, Y):
            fy_send(p, yo(d)).start()
        fc_send(p, y).start()

    def relay(p):
        for i in range(1, Y):
            fy_recv(p, yo(i)).wait_recv()
            fc_send(p, yo(i)).start()

    def arrive(p):
        for j in range(NH):
            a_send(p, j).wait_recv()
        forward(p)

    def norm(p):
        for i in range(Y):
            fc_recv(p, yo(i)).wait_recv()
        wide = x_all[span(p)].astype(F32)
        scale = lax.rsqrt(jnp.mean(wide * wide, axis=1, keepdims=True) + 1e-06)
        xn[span(p)] = (wide * scale * gain[...]).astype(BF16)

    TN = min(256, FL)
    NT = FL // TN

    def hidden(g, hooks):
        first, places = groups[g]
        m = len(places) * C

        @pl.loop(0, NT)
        def _(n):
            nn = pl.ds(pl.multiple_of(n * TN, TN), TN)
            gate = jnp.dot(xn[first : first + m], wg[:, nn], preferred_element_type=F32)
            up = jnp.dot(xn[first : first + m], wu[:, nn], preferred_element_type=F32)
            act[0:m, nn] = (gate / (1.0 + jnp.exp(-gate)) * up).astype(BF16)
            for i in range(NT):
                todo = hooks[i * len(hooks) // NT : (i + 1) * len(hooks) // NT]
                if todo:

                    @pl.when(n == i)
                    def _(todo=todo):
                        for hook in todo:
                            hook()

    def c2(g, yy):
        m = len(groups[g][1]) * C
        return remote(
            yp.at[g, pl.ds(0, m), cols(tp_of(yy, oc))],
            rc2.at[g, yy, pl.ds(0, m)],
            c2_s.at[g, yy],
            c2_r.at[g, yy],
            tp=tp_of(y, oc),
        )

    def down_block(g, tt):
        m = len(groups[g][1]) * C
        yp[g, 0:m, cols(tt)] = jnp.dot(
            act[0:m], wd[:, cols(tt)], preferred_element_type=F32
        ).astype(BF16)

    def y2_send(p, yy):
        g = group(p)
        return remote(
            sb2.at[g, yy, local(p)],
            ry2.at[g, y, local(p)],
            y2_s.at[p, yy],
            y2_r.at[p, y],
            tp=tp_of(yy, c),
        )

    def y2_recv(p, yy):
        g = group(p)
        return remote(
            sb2.at[g, yy, local(p)],
            ry2.at[g, yy, local(p)],
            y2_s.at[p, yy],
            y2_r.at[p, yy],
            tp=tp_of(yy, c),
        )

    back = (list(range(2, Z)) + [1, Z, 0], far[1:] + far[:1])

    def pair_sum(g, d):
        yy = yo(d)
        c2(g, yy).wait_recv()
        for p in back[g]:
            sb2[g, yy, local(p)] = (
                yp[g, local(p), cols(tp_of(yy, c))].astype(F32)
                + rc2[g, yy, local(p)].astype(F32)
            ).astype(BF16)
            y2_send(p, yy).start()

    def down(g):
        held = None
        for d in turns:
            down_block(g, tp_of(yo(d), oc))
            c2(g, yo(d)).start()
            if held is not None:
                pair_sum(g, held)
            down_block(g, tp_of(yo(d), c))
            held = d
        c2(g, y).wait_recv()

    def b_send(p):
        e = peer(p)
        return remote(rb.at[span(p)], ret.at[rows(me)], b_s.at[p], b_r.at[p], sp=e)

    def b_recv(p):
        e = peer(p)
        return remote(rb.at[span(p)], ret.at[rows(e)], b_s.at[p], b_r.at[p], sp=e)

    def send_back(p):
        g = group(p)
        total = yp[g, local(p), cols(t)].astype(F32) + rc2[g, y, local(p)].astype(F32)
        for d in range(1, Y):
            y2_recv(p, yo(d)).wait_recv()
            total = total + ry2[g, yo(d), local(p)].astype(F32)
        if p:
            rb[span(p)] = total.astype(BF16)
            b_send(p).start()
        else:
            ret[rows(me)] = total.astype(BF16)

    def later(f, *args):
        return lambda: f(*args)

    arrivals = [Z] + list(range(1, Z))
    forward(0)
    due = [0]
    for i, p in enumerate(arrivals):
        arrive(p)
        due.append(p)
        if i:
            relay(due.pop(0))
    for p in far[:1]:
        arrive(p)
    while len(due) > 1:
        relay(due.pop(0))
    norm(0)
    for p in arrivals[:-1]:
        norm(p)
    relay(due.pop(0))
    for p in far[1:2]:
        arrive(p)
    norm(arrivals[-1])
    loads[9].wait()
    loads[10].wait()
    hidden(0, [later(arrive, p) for p in far[2:]] + [later(relay, p) for p in far[:2]])
    loads[11].wait()
    for p in far[2:]:
        relay(p)
    down(0)
    for p in far:
        norm(p)
    hidden(1, [])
    down(1)
    for p in back[0] + back[1]:
        send_back(p)

    for p in range(1, S):
        b_recv(p).wait_recv()

    mix0 = jnp.dot(picker(slot0).astype(BF16), ret[...], preferred_element_type=F32)
    mix1 = jnp.dot(picker(slot1).astype(BF16), ret[...], preferred_element_type=F32)
    o_all[:, cols(t)] = (
        mixed[...].astype(F32) + (column(rw[0:1, :]) * mix0 + column(rw[1:2, :]) * mix1)
    ).astype(BF16)

    def gy_send(yy):
        ref = o_all.at[:, cols(t)]
        return remote(ref, ref, gy_s.at[yy], gy_r.at[y], tp=tp_of(yy, c))

    def gy_recv(yy):
        ref = o_all.at[:, cols(tp_of(yy, c))]
        return remote(ref, ref, gy_s.at[yy], gy_r.at[yy], tp=tp_of(yy, c))

    def gc_send(yy):
        at = cols(tp_of(yy, c))
        return remote(
            o_all.at[:, at], out_hbm.at[:, at], gc_s.at[yy], gc_r.at[yy], tp=tp_of(y, oc)
        )

    def gc_recv(yy):
        at = cols(tp_of(yy, oc))
        return remote(
            o_all.at[:, at], out_hbm.at[:, at], gc_s.at[yy], gc_r.at[yy], tp=tp_of(y, oc)
        )

    def write(yy):
        at = cols(tp_of(yy, c))
        return pltpu.make_async_copy(o_all.at[:, at], out_hbm.at[:, at], o_sem.at[yy])

    for d in range(1, Y):
        gy_send(yo(d)).start()
    gc_send(y).start()
    write(y).start()
    for d in range(1, Y):
        gy_recv(yo(d)).wait_recv()
        gc_send(yo(d)).start()
        write(yo(d)).start()

    @pl.when(me < S - 1)
    def _():
        for copy in halo_copies:
            copy.wait_send()

    for d in range(Y):
        c1(yo(d)).wait_send()
        for g in range(2):
            c2(g, yo(d)).wait_send()
    for p in range(S):
        if p:
            for j in range(NH):
                a_send(p, j).wait_send()
            b_send(p).wait_send()
        for d in range(Y):
            fc_send(p, yo(d)).wait_send()
        for d in range(1, Y):
            fy_send(p, yo(d)).wait_send()
            y2_send(p, yo(d)).wait_send()
    for d in range(1, Y):
        for j in range(NH):
            y1_send(yo(d), j).wait_send()
        gy_send(yo(d)).wait_send()
    for d in range(Y):
        gc_recv(yo(d)).wait_recv()
        gc_send(yo(d)).wait_send()
        write(yo(d)).wait()


def per_device(
    S,
    T,
    queries,
    key_rows,
    value_rows,
    sink_logits,
    out_weight,
    residual,
    norm_gain,
    routes,
    route_weights,
    gate_weight,
    up_weight,
    down_weight,
):
    R, D = residual.shape
    HW = queries.shape[1]
    Y = T // CORES
    W = D // T
    C = 2 * R * TOP // S
    Z = S // 2
    M = (Z + 1) * C
    FL = gate_weight.shape[2]
    NH = 2 if W % 256 == 0 else 1
    hbm = pl.BlockSpec(memory_space=pl.ANY)
    dma = pltpu.SemaphoreType.DMA
    v = pltpu.VMEM
    return pl.pallas_call(
        functools.partial(kernel, S, T),
        out_shape=jax.ShapeDtypeStruct((R, D), BF16),
        in_specs=[hbm] * 12,
        out_specs=hbm,
        scratch_shapes=[
            v((1, sink_logits.shape[0]), F32),
            v(queries.shape, BF16),
            v(key_rows.shape, BF16),
            v(value_rows.shape, BF16),
            v((R, W), BF16),
            v((1, D), F32),
            v((TOP, R), jnp.int32),
            v((TOP, R), F32),
            v(out_weight.shape, BF16),
            v(gate_weight.shape[1:], BF16),
            v(up_weight.shape[1:], BF16),
            v(down_weight.shape[1:], BF16),
            v((2,) + key_rows.shape, BF16),
            v((R, HW), BF16),
            v((R, D), BF16),
            v((Y, R, W), BF16),
            v((Y, NH, R, W // NH), BF16),
            v((Y, NH, R, W // NH), BF16),
            v((R, W), BF16),
            v((S * C, W), BF16),
            v((S * C, D), BF16),
            v((S * C, D), BF16),
            v((M, FL), BF16),
            v((2, M, D), BF16),
            v((2, Y, M, W), BF16),
            v((2, Y, M, W), BF16),
            v((2, Y, M, W), BF16),
            v((S * C, W), BF16),
            v((S * C, W), BF16),
            v((R, D), BF16),
            dma((12,)),
            dma((2,)),
            dma((2,)),
            dma((Y,)),
            dma((Y,)),
            dma((Y, NH)),
            dma((Y, NH)),
            dma((S, NH)),
            dma((S, NH)),
            dma((S, Y)),
            dma((S, Y)),
            dma((S, Y)),
            dma((S, Y)),
            dma((2, Y)),
            dma((2, Y)),
            dma((S, Y)),
            dma((S, Y)),
            dma((S,)),
            dma((S,)),
            dma((Y,)),
            dma((Y,)),
            dma((Y,)),
            dma((Y,)),
            dma((Y,)),
        ],
        compiler_params=pltpu.CompilerParams(
            collective_id=0, has_side_effects=True, vmem_limit_bytes=60 * 1024 * 1024
        ),
        name="layer",
    )(
        sink_logits.reshape(1, -1),
        queries,
        key_rows,
        value_rows,
        residual,
        norm_gain.reshape(1, D),
        routes.T,
        route_weights.T,
        out_weight,
        gate_weight,
        up_weight,
        down_weight,
    )


def solution(mesh):
    placed = (
        P("sp", "tp"),
        P("sp", "tp"),
        P("sp", "tp"),
        P("tp"),
        P("tp", None),
        P("sp", None),
        P(),
        P("sp", None),
        P("sp", None),
        P("sp", None, "tp"),
        P("sp", None, "tp"),
        P("sp", "tp", None),
    )
    return jax.shard_map(
        functools.partial(per_device, mesh.shape["sp"], mesh.shape["tp"]),
        mesh=mesh,
        in_specs=placed,
        out_specs=P("sp", None),
        check_vma=False,
    )
```

time: 71.2 us -> 68.8 us (0.966); the launches traced: 70.1 us -> 68.6 us
  Pallas kernels: 68.3 us -> 66.7 us
    pallas_call x1, Pallas kernels: 68.3 us -> 66.7 us  [per_device(): pl.pallas_call(functools.partial(kernel, S, T), out_shape=jax.ShapeDtypeS...]
where the time goes in v1:
time: 68.8 us; the launch traced here: 68.6 us
  Pallas kernels  66.7 us (97%)
  local copies, waits for them, and re-layouts  1.88 us (3%)
    pallas_call x1, Pallas kernels, per_device(): pl.pallas_call(functools.partial(kernel, S, T), out_shape=jax.ShapeDtypeS...  66.7 us
    unnamed x1, local copies, waits for them, and re-layouts  1.88 us

profile of v1, /device:TPU:0, one launch (start us, length us, event | category | flops | bytes accessed | tf_op | source)
XLA Modules:
  0.0 68.6 jit_solution(807547272554399361)
XLA Ops:
  0.0 66.7 %layer.1 = bf16[128,2048]{1,0:T(8,128)(2,1)} custom-call(f32[1,8]{1,0:T(1,128)} %bitcast.7, bf16[128,512]{1,0:T(8,128)(2,1)} %q_hbm.1, bf16[128,256]{1,0:T(8,128)(2,1)} %k_hbm.1, bf16[128,256]{1,0:T(8,128)(2,1)} %v_hbm.1, bf16[128,2048]{1,0:T(8,128)(2,1)} %res_hbm.1, f32[1,2048]{1,0:T(1,128)} %bitcast.4, s32[2,128]{1,0:T(2,128)} %bitcast.5, ...), custom_call_target="tpu_custom_call" | custom-call | tf_op jit(solution)/shard_map/layer/pallas_call | solution.py:632
  66.8 1.9 %copy.14 = bf16[128,2048]{1,0:T(8,128)(2,1)} copy(bf16[128,2048]{1,0:T(8,128)(2,1)} %layer.1) | data formatting | bytes 1048576

commit v2 on v1

--- a/solution.py
+++ b/solution.py
@@ -32,7 +32,7 @@
     wg_hbm,
     wu_hbm,
     wd_hbm,
-    out_hbm,
+    out,
     sink,
     q,
     k,
@@ -62,31 +62,19 @@
     ry2,
     rb,
     ret,
-    o_all,
     w_sem,
-    halo_s,
+    sent,
     halo_r,
-    c1_s,
     c1_r,
-    y1_s,
     y1_r,
-    a_s,
     a_r,
-    fy_s,
     fy_r,
-    fc_s,
     fc_r,
-    c2_s,
     c2_r,
-    y2_s,
     y2_r,
-    b_s,
     b_r,
-    gy_s,
     gy_r,
-    gc_s,
     gc_r,
-    o_sem,
 ):
     R, W = res.shape
     D = W * T
@@ -98,7 +86,8 @@
     Z = S // 2
     NEAR = (Z + 1) * C
     FL = wg.shape[1]
-    NH = y1_s.shape[1]
+    NH = y1_r.shape[1]
+    HALO, C1, Y1, A, FY, FC, C2, Y2, B, GY, GC = (sent.at[i] for i in range(11))
     HW = W // NH
 
     me = lax.axis_index("sp")
@@ -123,6 +112,9 @@
 
     def yo(d):
         return (y + d) % Y
+
+    def seen(d):
+        return Y - d - 1
 
     def remote(src, dst, ss, rs, **dev):
         return pltpu.make_async_remote_copy(
@@ -191,7 +183,7 @@
     pl.semaphore_wait(barrier, S - 1 + Y)
 
     halo_copies = [
-        remote(src, halo.at[i], halo_s.at[i], halo_r.at[i], sp=jnp.minimum(me + 1, S - 1))
+        remote(src, halo.at[i], HALO, halo_r.at[i], sp=jnp.minimum(me + 1, S - 1))
         for i, src in enumerate((k, v))
     ]
 
@@ -226,18 +218,14 @@
         slope = base * np.float32(2.0 ** (-8.0 * (h + 1) / (H * T)))
         return jnp.where(ok, raw * HEAD_DIM**-0.5 - slope * dist, -jnp.inf)
 
-    own = []
-    for h in range(H):
-        s_own = scores(h, k[:, head(h)[1]], dist_own, ok_own)
-        top = jnp.max(s_own, axis=1, keepdims=True)
-        e_own = jnp.exp(s_own - top)
-        own.append(
-            (
-                top,
-                jnp.sum(e_own, axis=1, keepdims=True),
-                jnp.dot(e_own.astype(BF16), v[:, head(h)[1]], preferred_element_type=F32),
-            )
-        )
+    s_own = [scores(h, k[:, head(h)[1]], dist_own, ok_own) for h in range(H)]
+    top = [jnp.max(a, axis=1, keepdims=True) for a in s_own]
+    e_own = [jnp.exp(a - b) for a, b in zip(s_own, top)]
+    weight = [jnp.sum(a, axis=1, keepdims=True) for a in e_own]
+    mix_own = [
+        jnp.dot(a.astype(BF16), v[:, head(h)[1]], preferred_element_type=F32)
+        for h, a in enumerate(e_own)
+    ]
 
     def column(row):
         return jnp.broadcast_to(row, (R, R)).T[:, 0:1]
@@ -267,26 +255,33 @@
 
     @pl.when(me > 0)
     def _():
-        for copy in halo_copies:
-            copy.wait_recv()
+        halo_copies[0].wait_recv()
 
     @pl.when(me == 0)
     def _():
         halo[...] = jnp.zeros_like(halo)
 
+    s_old = [scores(h, halo[0, :, head(h)[1]], dist_old, ok_old) for h in range(H)]
+    peak = [jnp.maximum(a, jnp.max(b, axis=1, keepdims=True)) for a, b in zip(top, s_old)]
+    shrink = [jnp.exp(a - b) for a, b in zip(top, peak)]
+    e_old = [jnp.exp(a - b) for a, b in zip(s_old, peak)]
+    total = [
+        a * b + jnp.sum(e, axis=1, keepdims=True) for a, b, e in zip(weight, shrink, e_old)
+    ]
+    keep = [
+        1.0 / (a + jnp.exp(sink[0:1, h : h + 1] - b)) for h, (a, b) in enumerate(zip(total, peak))
+    ]
+
+    @pl.when(me > 0)
+    def _():
+        halo_copies[1].wait_recv()
+
+    mix_old = [
+        jnp.dot(a.astype(BF16), halo[1, :, head(h)[1]], preferred_element_type=F32)
+        for h, a in enumerate(e_old)
+    ]
     for h in range(H):
-        hc, kc = head(h)
-        top, weight, mix = own[h]
-        s_old = scores(h, halo[0, :, kc], dist_old, ok_old)
-        peak = jnp.maximum(top, jnp.max(s_old, axis=1, keepdims=True))
-        shrink = jnp.exp(top - peak)
-        e_old = jnp.exp(s_old - peak)
-        total = weight * shrink + jnp.sum(e_old, axis=1, keepdims=True)
-        mix = mix * shrink + jnp.dot(
-            e_old.astype(BF16), halo[1, :, kc], preferred_element_type=F32
-        )
-        keep = 1.0 / (total + jnp.exp(sink[0:1, h : h + 1] - peak))
-        att[:, hc] = (mix * keep).astype(BF16)
+        att[:, head(h)[0]] = ((mix_own[h] * shrink[h] + mix_old[h]) * keep[h]).astype(BF16)
 
     for load in loads[5:9]:
         load.wait()
@@ -298,18 +293,18 @@
 
     def c1(yy):
         return remote(
-            pp.at[:, cols(tp_of(yy, oc))], rc1.at[yy], c1_s.at[yy], c1_r.at[yy], tp=tp_of(y, oc)
-        )
-
-    def y1_send(yy, j):
+            pp.at[:, cols(tp_of(yy, oc))], rc1.at[yy], C1, c1_r.at[yy], tp=tp_of(y, oc)
+        )
+
+    def y1_send(d, j):
+        yy = yo(d)
         return remote(
-            sb1.at[yy, j], ry1.at[y, j], y1_s.at[yy, j], y1_r.at[y, j], tp=tp_of(yy, c)
-        )
-
-    def y1_recv(yy, j):
-        return remote(
-            sb1.at[yy, j], ry1.at[yy, j], y1_s.at[yy, j], y1_r.at[yy, j], tp=tp_of(yy, c)
-        )
+            sb1.at[yy, j], ry1.at[y, j], Y1, y1_r.at[seen(d), j], tp=tp_of(yy, c)
+        )
+
+    def y1_recv(d, j):
+        yy = yo(d)
+        return remote(sb1.at[yy, j], ry1.at[yy, j], Y1, y1_r.at[d - 1, j], tp=tp_of(yy, c))
 
     turns = list(range(1, Y)) + [0]
 
@@ -327,68 +322,66 @@
             sb1[yo(d), j] = (
                 pp[:, part(tp_of(yo(d), c), j)].astype(F32) + rc1[yo(d), :, half(j)].astype(F32)
             ).astype(BF16)
-            y1_send(yo(d), j).start()
+            y1_send(d, j).start()
     c1(y).wait_recv()
 
     def a_send(p, j):
         e = peer(p)
         return remote(
-            picked.at[rows(e), half(j)],
-            x_all.at[span(p), part(t, j)],
-            a_s.at[p, j],
-            a_r.at[p, j],
-            sp=e,
-        )
-
-    def fy_send(p, yy):
+            picked.at[rows(e), half(j)], x_all.at[span(p), part(t, j)], A, a_r.at[p], sp=e
+        )
+
+    def a_recv(p):
+        e = peer(p)
+        return remote(picked.at[rows(e)], x_all.at[span(p), cols(t)], A, a_r.at[p], sp=e)
+
+    def fy_send(p, d):
         ref = x_all.at[span(p), cols(t)]
-        return remote(ref, ref, fy_s.at[p, yy], fy_r.at[p, y], tp=tp_of(yy, c))
-
-    def fy_recv(p, yy):
-        ref = x_all.at[span(p), cols(tp_of(yy, c))]
-        return remote(ref, ref, fy_s.at[p, yy], fy_r.at[p, yy], tp=tp_of(yy, c))
-
-    def fc_send(p, yy):
-        ref = x_all.at[span(p), cols(tp_of(yy, c))]
-        return remote(ref, ref, fc_s.at[p, yy], fc_r.at[p, yy], tp=tp_of(y, oc))
-
-    def fc_recv(p, yy):
-        ref = x_all.at[span(p), cols(tp_of(yy, oc))]
-        return remote(ref, ref, fc_s.at[p, yy], fc_r.at[p, yy], tp=tp_of(y, oc))
-
-    outward = [Z] + list(range(1, Z)) + far
+        return remote(ref, ref, FY, fy_r.at[p, seen(d)], tp=tp_of(yo(d), c))
+
+    def fy_recv(p, d):
+        ref = x_all.at[span(p), cols(tp_of(yo(d), c))]
+        return remote(ref, ref, FY, fy_r.at[p, d - 1], tp=tp_of(yo(d), c))
+
+    def fc_send(p, d):
+        ref = x_all.at[span(p), cols(tp_of(yo(d), c))]
+        return remote(ref, ref, FC, fc_r.at[p], tp=tp_of(y, oc))
+
+    def fc_recv(p):
+        ref = x_all.at[span(p), pl.ds(0, Y * W)]
+        return remote(ref, ref, FC, fc_r.at[p], tp=tp_of(y, oc))
+
+    arrivals = [Z] + list(range(1, Z))
 
     for j in range(NH):
         head_sum = pp[:, part(t, j)].astype(F32) + rc1[y, :, half(j)].astype(F32)
         for d in range(1, Y):
-            y1_recv(yo(d), j).wait_recv()
+            y1_recv(d, j).wait_recv()
             head_sum = head_sum + ry1[yo(d), j].astype(F32)
         mixed[:, half(j)] = (res[:, half(j)].astype(F32) + head_sum).astype(BF16)
         picked[:, half(j)] = jnp.dot(
             both, mixed[:, half(j)], preferred_element_type=F32
         ).astype(BF16)
-        for p in outward:
+        for p in arrivals:
             a_send(p, j).start()
     x_all[span(0), cols(t)] = picked[rows(me)]
 
     def forward(p):
         for d in range(1, Y):
-            fy_send(p, yo(d)).start()
-        fc_send(p, y).start()
+            fy_send(p, d).start()
+        fc_send(p, 0).start()
 
     def relay(p):
-        for i in range(1, Y):
-            fy_recv(p, yo(i)).wait_recv()
-            fc_send(p, yo(i)).start()
+        for d in range(1, Y):
+            fy_recv(p, d).wait_recv()
+            fc_send(p, d).start()
 
     def arrive(p):
-        for j in range(NH):
-            a_send(p, j).wait_recv()
+        a_recv(p).wait_recv()
         forward(p)
 
     def norm(p):
-        for i in range(Y):
-            fc_recv(p, yo(i)).wait_recv()
+        fc_recv(p).wait_recv()
         wide = x_all[span(p)].astype(F32)
         scale = lax.rsqrt(jnp.mean(wide * wide, axis=1, keepdims=True) + 1e-06)
         xn[span(p)] = (wide * scale * gain[...]).astype(BF16)
@@ -420,7 +413,7 @@
         return remote(
             yp.at[g, pl.ds(0, m), cols(tp_of(yy, oc))],
             rc2.at[g, yy, pl.ds(0, m)],
-            c2_s.at[g, yy],
+            C2,
             c2_r.at[g, yy],
             tp=tp_of(y, oc),
         )
@@ -431,24 +424,20 @@
             act[0:m], wd[:, cols(tt)], preferred_element_type=F32
         ).astype(BF16)
 
-    def y2_send(p, yy):
-        g = group(p)
+    def y2_send(p, d):
+        g, yy = group(p), yo(d)
         return remote(
             sb2.at[g, yy, local(p)],
             ry2.at[g, y, local(p)],
-            y2_s.at[p, yy],
-            y2_r.at[p, y],
+            Y2,
+            y2_r.at[p, seen(d)],
             tp=tp_of(yy, c),
         )
 
-    def y2_recv(p, yy):
-        g = group(p)
+    def y2_recv(p, d):
+        g, yy = group(p), yo(d)
         return remote(
-            sb2.at[g, yy, local(p)],
-            ry2.at[g, yy, local(p)],
-            y2_s.at[p, yy],
-            y2_r.at[p, yy],
-            tp=tp_of(yy, c),
+            sb2.at[g, yy, local(p)], ry2.at[g, yy, local(p)], Y2, y2_r.at[p, d - 1], tp=tp_of(yy, c)
         )
 
     back = (list(range(2, Z)) + [1, Z, 0], far[1:] + far[:1])
@@ -461,7 +450,8 @@
                 yp[g, local(p), cols(tp_of(yy, c))].astype(F32)
                 + rc2[g, yy, local(p)].astype(F32)
             ).astype(BF16)
-            y2_send(p, yy).start()
+            if p:
+                y2_send(p, d).start()
 
     def down(g):
         held = None
@@ -476,17 +466,13 @@
 
     def b_send(p):
         e = peer(p)
-        return remote(rb.at[span(p)], ret.at[rows(me)], b_s.at[p], b_r.at[p], sp=e)
-
-    def b_recv(p):
-        e = peer(p)
-        return remote(rb.at[span(p)], ret.at[rows(e)], b_s.at[p], b_r.at[p], sp=e)
+        return remote(rb.at[span(p)], ret.at[rows(me)], B, b_r.at[0], sp=e)
 
     def send_back(p):
         g = group(p)
         total = yp[g, local(p), cols(t)].astype(F32) + rc2[g, y, local(p)].astype(F32)
         for d in range(1, Y):
-            y2_recv(p, yo(d)).wait_recv()
+            y2_recv(p, d).wait_recv()
             total = total + ry2[g, yo(d), local(p)].astype(F32)
         if p:
             rb[span(p)] = total.astype(BF16)
@@ -497,13 +483,16 @@
     def later(f, *args):
         return lambda: f(*args)
 
-    arrivals = [Z] + list(range(1, Z))
     forward(0)
     due = [0]
     for i, p in enumerate(arrivals):
         arrive(p)
         due.append(p)
-        if i:
+        if i == 0:
+            for f in far:
+                for j in range(NH):
+                    a_send(f, j).start()
+        else:
             relay(due.pop(0))
     for p in far[:1]:
         arrive(p)
@@ -527,78 +516,64 @@
         norm(p)
     hidden(1, [])
     down(1)
-    for p in back[0] + back[1]:
+    for d in range(1, Y):
+        y2_send(0, d).start()
+    for p in back[0][:-1] + back[1] + [0]:
         send_back(p)
 
-    for p in range(1, S):
-        b_recv(p).wait_recv()
-
-    mix0 = jnp.dot(picker(slot0).astype(BF16), ret[...], preferred_element_type=F32)
-    mix1 = jnp.dot(picker(slot1).astype(BF16), ret[...], preferred_element_type=F32)
-    o_all[:, cols(t)] = (
-        mixed[...].astype(F32) + (column(rw[0:1, :]) * mix0 + column(rw[1:2, :]) * mix1)
-    ).astype(BF16)
-
-    def gy_send(yy):
-        ref = o_all.at[:, cols(t)]
-        return remote(ref, ref, gy_s.at[yy], gy_r.at[y], tp=tp_of(yy, c))
-
-    def gy_recv(yy):
-        ref = o_all.at[:, cols(tp_of(yy, c))]
-        return remote(ref, ref, gy_s.at[yy], gy_r.at[yy], tp=tp_of(yy, c))
-
-    def gc_send(yy):
-        at = cols(tp_of(yy, c))
-        return remote(
-            o_all.at[:, at], out_hbm.at[:, at], gc_s.at[yy], gc_r.at[yy], tp=tp_of(y, oc)
-        )
-
-    def gc_recv(yy):
-        at = cols(tp_of(yy, oc))
-        return remote(
-            o_all.at[:, at], out_hbm.at[:, at], gc_s.at[yy], gc_r.at[yy], tp=tp_of(y, oc)
-        )
-
-    def write(yy):
-        at = cols(tp_of(yy, c))
-        return pltpu.make_async_copy(o_all.at[:, at], out_hbm.at[:, at], o_sem.at[yy])
-
-    for d in range(1, Y):
-        gy_send(yo(d)).start()
-    gc_send(y).start()
-    write(y).start()
-    for d in range(1, Y):
-        gy_recv(yo(d)).wait_recv()
-        gc_send(yo(d)).start()
-        write(yo(d)).start()
+    others = pl.ds(0, (S - 1) * C)
+    remote(rb.at[others], ret.at[others], B, b_r.at[0], sp=peer(1)).wait_recv()
+
+    def gy_send(d, j):
+        ref = out.at[:, part(t, j)]
+        return remote(ref, ref, GY, gy_r.at[seen(d), j], tp=tp_of(yo(d), c))
+
+    def gy_recv(d, j):
+        ref = out.at[:, part(tp_of(yo(d), c), j)]
+        return remote(ref, ref, GY, gy_r.at[d - 1, j], tp=tp_of(yo(d), c))
+
+    def gc_send(d, j):
+        ref = out.at[:, part(tp_of(yo(d), c), j)]
+        return remote(ref, ref, GC, gc_r.at[0], tp=tp_of(y, oc))
+
+    pick0 = picker(slot0).astype(BF16)
+    pick1 = picker(slot1).astype(BF16)
+    rw0 = column(rw[0:1, :])
+    rw1 = column(rw[1:2, :])
+    for j in range(NH):
+        mix0 = jnp.dot(pick0, ret[:, half(j)], preferred_element_type=F32)
+        mix1 = jnp.dot(pick1, ret[:, half(j)], preferred_element_type=F32)
+        out[:, part(t, j)] = (
+            mixed[:, half(j)].astype(F32) + (rw0 * mix0 + rw1 * mix1)
+        ).astype(BF16)
+        for d in range(1, Y):
+            gy_send(d, j).start()
+        gc_send(0, j).start()
 
     @pl.when(me < S - 1)
     def _():
-        for copy in halo_copies:
-            copy.wait_send()
-
-    for d in range(Y):
-        c1(yo(d)).wait_send()
-        for g in range(2):
-            c2(g, yo(d)).wait_send()
-    for p in range(S):
-        if p:
-            for j in range(NH):
-                a_send(p, j).wait_send()
-            b_send(p).wait_send()
-        for d in range(Y):
-            fc_send(p, yo(d)).wait_send()
+        remote(halo, halo, HALO, halo_r.at[0], sp=me + 1).wait_send()
+
+    def drain(ref, sem):
+        remote(ref, ref, sem, sem, tp=tp_of(y, oc)).wait_send()
+
+    drain(rc1, C1)
+    drain(sb1.at[pl.ds(0, Y - 1)], Y1)
+    drain(ret.at[others], A)
+    drain(x_all.at[:, pl.ds(0, (Y - 1) * W)], FY)
+    drain(x_all.at[:, pl.ds(0, Y * W)], FC)
+    drain(x_all.at[:, pl.ds(0, Y * W)], C2)
+    drain(x_all.at[:, pl.ds(0, (Y - 1) * W)], Y2)
+    drain(ret.at[others], B)
+
+    for j in range(NH):
         for d in range(1, Y):
-            fy_send(p, yo(d)).wait_send()
-            y2_send(p, yo(d)).wait_send()
-    for d in range(1, Y):
-        for j in range(NH):
-            y1_send(yo(d), j).wait_send()
-        gy_send(yo(d)).wait_send()
-    for d in range(Y):
-        gc_recv(yo(d)).wait_recv()
-        gc_send(yo(d)).wait_send()
-        write(yo(d)).wait()
+            gy_recv(d, j).wait_recv()
+            gc_send(d, j).start()
+    ours = out.at[:, pl.ds(0, Y * W)]
+    remote(ours, ours, GC, gc_r.at[0], tp=tp_of(y, oc)).wait_recv()
+    drain(ours, GC)
+    drain(out.at[:, pl.ds(0, (Y - 1) * W)], GY)
 
 
 def per_device(
@@ -631,9 +606,9 @@
     v = pltpu.VMEM
     return pl.pallas_call(
         functools.partial(kernel, S, T),
-        out_shape=jax.ShapeDtypeStruct((R, D), BF16),
+        out_shape=v((R, D), BF16),
         in_specs=[hbm] * 12,
-        out_specs=hbm,
+        out_specs=pl.BlockSpec(memory_space=v),
         scratch_shapes=[
             v((1, sink_logits.shape[0]), F32),
             v(queries.shape, BF16),
@@ -664,31 +639,19 @@
             v((2, Y, M, W), BF16),
             v((S * C, W), BF16),
             v((S * C, W), BF16),
-            v((R, D), BF16),
             dma((12,)),
-            dma((2,)),
+            dma((11,)),
             dma((2,)),
             dma((Y,)),
-            dma((Y,)),
-            dma((Y, NH)),
-            dma((Y, NH)),
-            dma((S, NH)),
-            dma((S, NH)),
-            dma((S, Y)),
-            dma((S, Y)),
-            dma((S, Y)),
-            dma((S, Y)),
+            dma((Y - 1, NH)),
+            dma((S,)),
+            dma((S, Y - 1)),
+            dma((S,)),
             dma((2, Y)),
-            dma((2, Y)),
-            dma((S, Y)),
-            dma((S, Y)),
-            dma((S,)),
-            dma((S,)),
-            dma((Y,)),
-            dma((Y,)),
-            dma((Y,)),
-            dma((Y,)),
-            dma((Y,)),
+            dma((S, Y - 1)),
+            dma((1,)),
+            dma((Y - 1, NH)),
+            dma((1,)),
         ],
         compiler_params=pltpu.CompilerParams(
             collective_id=0, has_side_effects=True, vmem_limit_bytes=60 * 1024 * 1024

time: 68.8 us -> 61.5 us (0.89)
  Pallas kernels: 66.7 us -> 60.5 us
  local copies, waits for them, and re-layouts: 1.88 us -> 0.8 us
    pallas_call x1, Pallas kernels: 66.7 us -> 60.5 us  [per_device(): pl.pallas_call(functools.partial(kernel, S, T), out_shape=v((R, D), BF16)...]
    unnamed x1, local copies, waits for them, and re-layouts: 1.88 us -> 0.8 us
where the time goes in v2:
time: 61.5 us; the launch traced here: 61.3 us
  Pallas kernels  60.5 us (98%)
  local copies, waits for them, and re-layouts  0.8 us (1%)
    pallas_call x1, Pallas kernels, per_device(): pl.pallas_call(functools.partial(kernel, S, T), out_shape=v((R, D), BF16)...  60.5 us

profile of v2, /device:TPU:0, one launch (start us, length us, event | category | flops | bytes accessed | tf_op | source)
XLA Modules:
  0.0 61.3 jit_solution(4197416396616754736)
XLA Ops:
  0.0 60.5 %layer.1 = bf16[128,2048]{1,0:T(8,128)(2,1)S(1)} custom-call(f32[1,8]{1,0:T(1,128)} %bitcast.7, bf16[128,512]{1,0:T(8,128)(2,1)} %q_hbm.1, bf16[128,256]{1,0:T(8,128)(2,1)} %k_hbm.1, bf16[128,256]{1,0:T(8,128)(2,1)} %v_hbm.1, bf16[128,2048]{1,0:T(8,128)(2,1)} %res_hbm.1, f32[1,2048]{1,0:T(1,128)} %bitcast.4, s32[2,128]{1,0:T(2,128)} %bitcast.5, ...), custom_call_target="tpu_custom_call" | custom-call | tf_op jit(solution)/shard_map/layer/pallas_call | solution.py:607
  60.6 0.8 %copy.14 = bf16[128,2048]{1,0:T(8,128)(2,1)} copy(bf16[128,2048]{1,0:T(8,128)(2,1)S(1)} %layer.1) | data formatting | bytes 1048576

commit v3 on v2

--- a/solution.py
+++ b/solution.py
@@ -84,11 +84,12 @@
     G = H // KV
     C = x_all.shape[0] // S
     Z = S // 2
-    NEAR = (Z + 1) * C
     FL = wg.shape[1]
     NH = y1_r.shape[1]
     HALO, C1, Y1, A, FY, FC, C2, Y2, B, GY, GC = (sent.at[i] for i in range(11))
     HW = W // NH
+    NF = gy_r.shape[1]
+    FW = W // NF
 
     me = lax.axis_index("sp")
     t = lax.axis_index("tp")
@@ -107,6 +108,12 @@
     def part(tt, j):
         return pl.ds(pl.multiple_of(tt * W + j * HW, HW), HW)
 
+    def wide(tt, f):
+        return pl.ds(pl.multiple_of(tt * W + f * FW, FW), FW)
+
+    def fold(f):
+        return pl.ds(f * FW, FW)
+
     def rows(s):
         return pl.ds(pl.multiple_of(s * C, C), C)
 
@@ -121,27 +128,27 @@
             src_ref=src, dst_ref=dst, send_sem=ss, recv_sem=rs, device_id=dev, device_id_type=MESH
         )
 
+    places = [(0, 0), (1, 0)] + [(0, d) for d in range(1, Z)] + [(1, d) for d in range(1, Z)]
+    split = min(3, Z + 1)
+    first = list(range(split))
+    second = list(range(split, Z + 1))
+    third = list(range(Z + 1, S))
+
     def peer(p):
+        parity, bits = places[p]
         zz = z
         bit = 1
         while bit < Z:
-            if (p % Z) // bit % 2:
+            if bits // bit % 2:
                 zz = zz + bit * (1 - 2 * (zz // bit % 2))
             bit *= 2
-        return 2 * zz + (x + p // Z) % 2
-
-    far = list(range(Z + 1, 2 * Z))
-    near = list(range(Z + 1))
-    groups = ((0, near), (NEAR, far))
+        return 2 * zz + (x + parity) % 2
 
     def span(p):
         return pl.ds(p * C, C)
 
-    def local(p):
-        return pl.ds((p if p <= Z else p - Z - 1) * C, C)
-
-    def group(p):
-        return 0 if p <= Z else 1
+    def block(group):
+        return pl.ds(group[0] * C, len(group) * C)
 
     barrier = pltpu.get_barrier_semaphore()
 
@@ -328,30 +335,36 @@
     def a_send(p, j):
         e = peer(p)
         return remote(
-            picked.at[rows(e), half(j)], x_all.at[span(p), part(t, j)], A, a_r.at[p], sp=e
-        )
-
-    def a_recv(p):
+            picked.at[rows(e), half(j)],
+            x_all.at[span(p), part(t, j)],
+            A,
+            a_r.at[p, j * NF // NH],
+            sp=e,
+        )
+
+    def a_fold(p, f):
         e = peer(p)
-        return remote(picked.at[rows(e)], x_all.at[span(p), cols(t)], A, a_r.at[p], sp=e)
-
-    def fy_send(p, d):
-        ref = x_all.at[span(p), cols(t)]
-        return remote(ref, ref, FY, fy_r.at[p, seen(d)], tp=tp_of(yo(d), c))
-
-    def fy_recv(p, d):
-        ref = x_all.at[span(p), cols(tp_of(yo(d), c))]
-        return remote(ref, ref, FY, fy_r.at[p, d - 1], tp=tp_of(yo(d), c))
-
-    def fc_send(p, d):
-        ref = x_all.at[span(p), cols(tp_of(yo(d), c))]
+        return remote(
+            picked.at[rows(e), fold(f)], x_all.at[span(p), wide(t, f)], A, a_r.at[p, f], sp=e
+        )
+
+    def fy_send(p, d, f):
+        ref = x_all.at[span(p), wide(t, f)]
+        return remote(ref, ref, FY, fy_r.at[p, seen(d), f], tp=tp_of(yo(d), c))
+
+    def fy_recv(p, d, f):
+        ref = x_all.at[span(p), wide(tp_of(yo(d), c), f)]
+        return remote(ref, ref, FY, fy_r.at[p, d - 1, f], tp=tp_of(yo(d), c))
+
+    def fc_send(p, d, f):
+        ref = x_all.at[span(p), wide(tp_of(yo(d), c), f)]
         return remote(ref, ref, FC, fc_r.at[p], tp=tp_of(y, oc))
 
     def fc_recv(p):
         ref = x_all.at[span(p), pl.ds(0, Y * W)]
         return remote(ref, ref, FC, fc_r.at[p], tp=tp_of(y, oc))
 
-    arrivals = [Z] + list(range(1, Z))
+    arrivals = list(range(1, Z + 1))
 
     for j in range(NH):
         head_sum = pp[:, part(t, j)].astype(F32) + rc1[y, :, half(j)].astype(F32)
@@ -366,19 +379,21 @@
             a_send(p, j).start()
     x_all[span(0), cols(t)] = picked[rows(me)]
 
-    def forward(p):
+    def forward(p, f):
         for d in range(1, Y):
-            fy_send(p, d).start()
-        fc_send(p, 0).start()
+            fy_send(p, d, f).start()
+        fc_send(p, 0, f).start()
 
     def relay(p):
-        for d in range(1, Y):
-            fy_recv(p, d).wait_recv()
-            fc_send(p, d).start()
+        for f in range(NF):
+            for d in range(1, Y):
+                fy_recv(p, d, f).wait_recv()
+                fc_send(p, d, f).start()
 
     def arrive(p):
-        a_recv(p).wait_recv()
-        forward(p)
+        for f in range(NF):
+            a_fold(p, f).wait_recv()
+            forward(p, f)
 
     def norm(p):
         fc_recv(p).wait_recv()
@@ -389,18 +404,17 @@
     TN = min(256, FL)
     NT = FL // TN
 
-    def hidden(g, hooks):
-        first, places = groups[g]
-        m = len(places) * C
+    def hidden(group, hooks):
+        at = block(group)
 
         @pl.loop(0, NT)
         def _(n):
             nn = pl.ds(pl.multiple_of(n * TN, TN), TN)
-            gate = jnp.dot(xn[first : first + m], wg[:, nn], preferred_element_type=F32)
-            up = jnp.dot(xn[first : first + m], wu[:, nn], preferred_element_type=F32)
-            act[0:m, nn] = (gate / (1.0 + jnp.exp(-gate)) * up).astype(BF16)
+            gate = jnp.dot(xn[at], wg[:, nn], preferred_element_type=F32)
+            up = jnp.dot(xn[at], wu[:, nn], preferred_element_type=F32)
+            act[at, nn] = (gate / (1.0 + jnp.exp(-gate)) * up).astype(BF16)
             for i in range(NT):
-                todo = hooks[i * len(hooks) // NT : (i + 1) * len(hooks) // NT]
+                todo = [hook for turn, hook in hooks if min(turn, NT - 1) == i]
                 if todo:
 
                     @pl.when(n == i)
@@ -408,143 +422,153 @@
                         for hook in todo:
                             hook()
 
-    def c2(g, yy):
-        m = len(groups[g][1]) * C
+    def c2(g, d):
+        at = block(groups[g])
         return remote(
-            yp.at[g, pl.ds(0, m), cols(tp_of(yy, oc))],
-            rc2.at[g, yy, pl.ds(0, m)],
-            C2,
-            c2_r.at[g, yy],
-            tp=tp_of(y, oc),
+            yp.at[at, cols(tp_of(yo(d), oc))], rc2.at[d, at], C2, c2_r.at[g, d], tp=tp_of(y, oc)
         )
 
     def down_block(g, tt):
-        m = len(groups[g][1]) * C
-        yp[g, 0:m, cols(tt)] = jnp.dot(
-            act[0:m], wd[:, cols(tt)], preferred_element_type=F32
-        ).astype(BF16)
-
-    def y2_send(p, d):
-        g, yy = group(p), yo(d)
+        at = block(groups[g])
+        yp[at, cols(tt)] = jnp.dot(act[at], wd[:, cols(tt)], preferred_element_type=F32).astype(
+            BF16
+        )
+
+    def y2_send(p, d, f):
         return remote(
-            sb2.at[g, yy, local(p)],
-            ry2.at[g, y, local(p)],
+            sb2.at[d - 1, span(p), fold(f)],
+            ry2.at[seen(d), span(p), fold(f)],
             Y2,
-            y2_r.at[p, seen(d)],
-            tp=tp_of(yy, c),
-        )
-
-    def y2_recv(p, d):
-        g, yy = group(p), yo(d)
+            y2_r.at[p, seen(d), f],
+            tp=tp_of(yo(d), c),
+        )
+
+    def y2_recv(p, d, f):
         return remote(
-            sb2.at[g, yy, local(p)], ry2.at[g, yy, local(p)], Y2, y2_r.at[p, d - 1], tp=tp_of(yy, c)
-        )
-
-    back = (list(range(2, Z)) + [1, Z, 0], far[1:] + far[:1])
+            sb2.at[d - 1, span(p), fold(f)],
+            ry2.at[d - 1, span(p), fold(f)],
+            Y2,
+            y2_r.at[p, d - 1, f],
+            tp=tp_of(yo(d), c),
+        )
+
+    groups = [g for g in (first, second, third) if g]
+    back = [g[:0:-1] + g[:1] if g is first else g[1:] + g[:1] for g in groups]
 
     def pair_sum(g, d):
-        yy = yo(d)
-        c2(g, yy).wait_recv()
+        c2(g, d).wait_recv()
         for p in back[g]:
-            sb2[g, yy, local(p)] = (
-                yp[g, local(p), cols(tp_of(yy, c))].astype(F32)
-                + rc2[g, yy, local(p)].astype(F32)
+            at = span(p)
+            sb2[d - 1, at] = (
+                yp[at, cols(tp_of(yo(d), c))].astype(F32) + rc2[d, at].astype(F32)
             ).astype(BF16)
-            if p:
-                y2_send(p, d).start()
-
-    def down(g):
+            for f in range(NF):
+                y2_send(p, d, f).start()
+
+    def down(g, hooks):
         held = None
+        hooks = list(hooks)
         for d in turns:
             down_block(g, tp_of(yo(d), oc))
-            c2(g, yo(d)).start()
+            c2(g, d).start()
             if held is not None:
                 pair_sum(g, held)
+            if hooks:
+                hooks.pop(0)()
             down_block(g, tp_of(yo(d), c))
-            held = d
-        c2(g, y).wait_recv()
-
-    def b_send(p):
+            if hooks:
+                hooks.pop(0)()
+            held = d or None
+        for hook in hooks:
+            hook()
+        c2(g, 0).wait_recv()
+
+    def b_send(p, f):
         e = peer(p)
-        return remote(rb.at[span(p)], ret.at[rows(me)], B, b_r.at[0], sp=e)
+        return remote(
+            rb.at[span(p), fold(f)], ret.at[rows(me), fold(f)], B, b_r.at[0], sp=e
+        )
 
     def send_back(p):
-        g = group(p)
-        total = yp[g, local(p), cols(t)].astype(F32) + rc2[g, y, local(p)].astype(F32)
-        for d in range(1, Y):
-            y2_recv(p, d).wait_recv()
-            total = total + ry2[g, yo(d), local(p)].astype(F32)
-        if p:
-            rb[span(p)] = total.astype(BF16)
-            b_send(p).start()
-        else:
-            ret[rows(me)] = total.astype(BF16)
+        at = span(p)
+        for f in range(NF):
+            total = yp[at, wide(t, f)].astype(F32) + rc2[0, at, fold(f)].astype(F32)
+            for d in range(1, Y):
+                y2_recv(p, d, f).wait_recv()
+                total = total + ry2[d - 1, at, fold(f)].astype(F32)
+            if p:
+                rb[at, fold(f)] = total.astype(BF16)
+                b_send(p, f).start()
+            else:
+                ret[rows(me), fold(f)] = total.astype(BF16)
 
     def later(f, *args):
         return lambda: f(*args)
 
-    forward(0)
-    due = [0]
+    for f in range(NF):
+        forward(0, f)
     for i, p in enumerate(arrivals):
         arrive(p)
-        due.append(p)
         if i == 0:
-            for f in far:
-                for j in range(NH):
-                    a_send(f, j).start()
-        else:
-            relay(due.pop(0))
-    for p in far[:1]:
-        arrive(p)
-    while len(due) > 1:
-        relay(due.pop(0))
-    norm(0)
-    for p in arrivals[:-1]:
+            for q in third:
+                for f in range(NF):
+                    a_fold(q, f).start()
+        elif p <= split:
+            relay(p - 2)
+    for p in range(min(split, Z) - 1, split):
+        relay(p)
+    for p in first:
         norm(p)
-    relay(due.pop(0))
-    for p in far[1:2]:
-        arrive(p)
-    norm(arrivals[-1])
     loads[9].wait()
     loads[10].wait()
-    hidden(0, [later(arrive, p) for p in far[2:]] + [later(relay, p) for p in far[:2]])
+    steps = [later(arrive, p) for p in third[:1]] + [later(relay, p) for p in second]
+    steps += [later(arrive, p) for p in third[1:2]]
+    hidden(first, [(i, step) for i, step in enumerate(steps)])
     loads[11].wait()
-    for p in far[2:]:
-        relay(p)
-    down(0)
-    for p in far:
+    if second:
+        for p in second:
+            norm(p)
+        steps = [later(arrive, p) for p in third[2:]] + [later(relay, p) for p in third[:-2]]
+        hidden(second, [(i, step) for i, step in enumerate(steps)])
+        down(1, [later(lambda: None), later(relay, third[-2])])
+    else:
+        for p in third[2:]:
+            arrive(p)
+        for p in third[:-1]:
+            relay(p)
+    down(0, [later(lambda: None), later(relay, third[-1])])
+    for p in third:
         norm(p)
-    hidden(1, [])
-    down(1)
-    for d in range(1, Y):
-        y2_send(0, d).start()
-    for p in back[0][:-1] + back[1] + [0]:
+    steps = [later(send_back, p) for p in back[1]] if second else []
+    hidden(third, [(2 * i + 1, step) for i, step in enumerate(steps)])
+    down(len(groups) - 1, [])
+    for p in back[0] + back[-1]:
         send_back(p)
 
     others = pl.ds(0, (S - 1) * C)
     remote(rb.at[others], ret.at[others], B, b_r.at[0], sp=peer(1)).wait_recv()
 
     def gy_send(d, j):
-        ref = out.at[:, part(t, j)]
+        ref = out.at[:, wide(t, j)]
         return remote(ref, ref, GY, gy_r.at[seen(d), j], tp=tp_of(yo(d), c))
 
     def gy_recv(d, j):
-        ref = out.at[:, part(tp_of(yo(d), c), j)]
+        ref = out.at[:, wide(tp_of(yo(d), c), j)]
         return remote(ref, ref, GY, gy_r.at[d - 1, j], tp=tp_of(yo(d), c))
 
     def gc_send(d, j):
-        ref = out.at[:, part(tp_of(yo(d), c), j)]
+        ref = out.at[:, wide(tp_of(yo(d), c), j)]
         return remote(ref, ref, GC, gc_r.at[0], tp=tp_of(y, oc))
 
     pick0 = picker(slot0).astype(BF16)
     pick1 = picker(slot1).astype(BF16)
     rw0 = column(rw[0:1, :])
     rw1 = column(rw[1:2, :])
-    for j in range(NH):
-        mix0 = jnp.dot(pick0, ret[:, half(j)], preferred_element_type=F32)
-        mix1 = jnp.dot(pick1, ret[:, half(j)], preferred_element_type=F32)
-        out[:, part(t, j)] = (
-            mixed[:, half(j)].astype(F32) + (rw0 * mix0 + rw1 * mix1)
+    for j in range(NF):
+        mix0 = jnp.dot(pick0, ret[:, fold(j)], preferred_element_type=F32)
+        mix1 = jnp.dot(pick1, ret[:, fold(j)], preferred_element_type=F32)
+        out[:, wide(t, j)] = (
+            mixed[:, fold(j)].astype(F32) + (rw0 * mix0 + rw1 * mix1)
         ).astype(BF16)
         for d in range(1, Y):
             gy_send(d, j).start()
@@ -566,7 +590,7 @@
     drain(x_all.at[:, pl.ds(0, (Y - 1) * W)], Y2)
     drain(ret.at[others], B)
 
-    for j in range(NH):
+    for j in range(NF):
         for d in range(1, Y):
             gy_recv(d, j).wait_recv()
             gc_send(d, j).start()
@@ -597,10 +621,9 @@
     Y = T // CORES
     W = D // T
     C = 2 * R * TOP // S
-    Z = S // 2
-    M = (Z + 1) * C
     FL = gate_weight.shape[2]
-    NH = 2 if W % 256 == 0 else 1
+    NH = 4 if W % 512 == 0 else 1
+    NF = 2 if W % 256 == 0 else 1
     hbm = pl.BlockSpec(memory_space=pl.ANY)
     dma = pltpu.SemaphoreType.DMA
     v = pltpu.VMEM
@@ -632,11 +655,11 @@
             v((S * C, W), BF16),
             v((S * C, D), BF16),
             v((S * C, D), BF16),
-            v((M, FL), BF16),
-            v((2, M, D), BF16),
-            v((2, Y, M, W), BF16),
-            v((2, Y, M, W), BF16),
-            v((2, Y, M, W), BF16),
+            v((S * C, FL), BF16),
+            v((S * C, D), BF16),
+            v((Y, S * C, W), BF16),
+            v((Y - 1, S * C, W), BF16),
+            v((Y - 1, S * C, W), BF16),
             v((S * C, W), BF16),
             v((S * C, W), BF16),
             dma((12,)),
@@ -644,13 +667,13 @@
             dma((2,)),
             dma((Y,)),
             dma((Y - 1, NH)),
+            dma((S, NF)),
+            dma((S, Y - 1, NF)),
             dma((S,)),
-            dma((S, Y - 1)),
-            dma((S,)),
-            dma((2, Y)),
-            dma((S, Y - 1)),
+            dma((3, Y)),
+            dma((S, Y - 1, NF)),
             dma((1,)),
-            dma((Y - 1, NH)),
+            dma((Y - 1, NF)),
             dma((1,)),
         ],
         compiler_params=pltpu.CompilerParams(

time: 61.5 us -> 58.5 us (0.951)
  Pallas kernels: 60.5 us -> 57.6 us
    pallas_call x1, Pallas kernels: 60.5 us -> 57.6 us  [per_device(): pl.pallas_call(functools.partial(kernel, S, T), out_shape=v((R, D), BF16)...]
where the time goes in v3:
time: 58.5 us; the launch traced here: 58.4 us
  Pallas kernels  57.6 us (98%)
  local copies, waits for them, and re-layouts  0.8 us (1%)
    pallas_call x1, Pallas kernels, per_device(): pl.pallas_call(functools.partial(kernel, S, T), out_shape=v((R, D), BF16)...  57.6 us

profile of v3, /device:TPU:0, one launch (start us, length us, event | category | flops | bytes accessed | tf_op | source)
XLA Modules:
  0.0 58.4 jit_solution(1390532919712023759)
XLA Ops:
  0.0 57.6 %layer.1 = bf16[128,2048]{1,0:T(8,128)(2,1)S(1)} custom-call(f32[1,8]{1,0:T(1,128)} %bitcast.7, bf16[128,512]{1,0:T(8,128)(2,1)} %q_hbm.1, bf16[128,256]{1,0:T(8,128)(2,1)} %k_hbm.1, bf16[128,256]{1,0:T(8,128)(2,1)} %v_hbm.1, bf16[128,2048]{1,0:T(8,128)(2,1)} %res_hbm.1, f32[1,2048]{1,0:T(1,128)} %bitcast.4, s32[2,128]{1,0:T(2,128)} %bitcast.5, ...), custom_call_target="tpu_custom_call" | custom-call | tf_op jit(solution)/shard_map/layer/pallas_call | solution.py:630
  57.6 0.8 %copy.14 = bf16[128,2048]{1,0:T(8,128)(2,1)} copy(bf16[128,2048]{1,0:T(8,128)(2,1)S(1)} %layer.1) | data formatting | bytes 1048576

commit v4 on v3

--- a/solution.py
+++ b/solution.py
@@ -63,6 +63,7 @@
     rb,
     ret,
     w_sem,
+    met,
     sent,
     halo_r,
     c1_r,
@@ -152,12 +153,28 @@
 
     barrier = pltpu.get_barrier_semaphore()
 
-    @pl.loop(1, S)
-    def _(d):
-        pl.semaphore_signal(
-            barrier, inc=1, device_id={"sp": (me + d) % S}, device_id_type=MESH
-        )
-
+    def greet(sem, step):
+        for ok, e in ((me >= step, me - step), (me + step < S, me + step)):
+
+            @pl.when(ok)
+            def _(e=e):
+                pl.semaphore_signal(sem, inc=1, device_id={"sp": e}, device_id_type=MESH)
+
+    def greeted(sem, step, more=0):
+        both = jnp.minimum(me // step, 1) + jnp.minimum((S - 1 - me) // step, 1)
+        pl.semaphore_wait(sem, both + more)
+
+    reach = [1]
+    while 2 * reach[-1] < S:
+        reach.append(2 * reach[-1])
+
+    def meet(i):
+        if i:
+            greeted(met.at[i - 1], reach[i - 1])
+        if i < len(reach):
+            greet(met.at[i], reach[i])
+
+    greet(barrier, 1)
     for d in range(1, Y):
         pl.semaphore_signal(
             barrier, inc=1, device_id={"tp": tp_of(yo(d), c)}, device_id_type=MESH
@@ -187,7 +204,7 @@
         load.start()
     loads[0].wait()
     loads[1].wait()
-    pl.semaphore_wait(barrier, S - 1 + Y)
+    greeted(barrier, 1, Y)
 
     halo_copies = [
         remote(src, halo.at[i], HALO, halo_r.at[i], sp=jnp.minimum(me + 1, S - 1))
@@ -199,6 +216,7 @@
         for copy in halo_copies:
             copy.start()
 
+    meet(0)
     for load in loads[2:5]:
         load.wait()
 
@@ -233,6 +251,8 @@
         jnp.dot(a.astype(BF16), v[:, head(h)[1]], preferred_element_type=F32)
         for h, a in enumerate(e_own)
     ]
+
+    meet(1)
 
     def column(row):
         return jnp.broadcast_to(row, (R, R)).T[:, 0:1]
@@ -290,6 +310,7 @@
     for h in range(H):
         att[:, head(h)[0]] = ((mix_own[h] * shrink[h] + mix_old[h]) * keep[h]).astype(BF16)
 
+    meet(2)
     for load in loads[5:9]:
         load.wait()
 
@@ -318,19 +339,24 @@
     def half(j):
         return slice(j * HW, (j + 1) * HW)
 
-    for d in turns:
+    for d in turns[:-1]:
         project(tp_of(yo(d), oc))
         c1(yo(d)).start()
-    for d in turns:
+    for d in turns[:-1]:
         project(tp_of(yo(d), c))
-    for d in range(1, Y):
+    for d in turns[:-1]:
         c1(yo(d)).wait_recv()
         for j in range(NH):
             sb1[yo(d), j] = (
                 pp[:, part(tp_of(yo(d), c), j)].astype(F32) + rc1[yo(d), :, half(j)].astype(F32)
             ).astype(BF16)
             y1_send(d, j).start()
+    project(tp_of(y, oc))
+    c1(y).start()
+    project(t)
     c1(y).wait_recv()
+    for i in range(3, len(reach) + 1):
+        meet(i)
 
     def a_send(p, j):
         e = peer(p)
@@ -465,23 +491,12 @@
             for f in range(NF):
                 y2_send(p, d, f).start()
 
-    def down(g, hooks):
-        held = None
-        hooks = list(hooks)
-        for d in turns:
+    def down(g, turn):
+        for d in turn:
             down_block(g, tp_of(yo(d), oc))
             c2(g, d).start()
-            if held is not None:
-                pair_sum(g, held)
-            if hooks:
-                hooks.pop(0)()
+        for d in turn:
             down_block(g, tp_of(yo(d), c))
-            if hooks:
-                hooks.pop(0)()
-            held = d or None
-        for hook in hooks:
-            hook()
-        c2(g, 0).wait_recv()
 
     def b_send(p, f):
         e = peer(p)
@@ -525,23 +540,42 @@
     steps += [later(arrive, p) for p in third[1:2]]
     hidden(first, [(i, step) for i, step in enumerate(steps)])
     loads[11].wait()
+    last = len(groups) - 1
     if second:
         for p in second:
             norm(p)
         steps = [later(arrive, p) for p in third[2:]] + [later(relay, p) for p in third[:-2]]
         hidden(second, [(i, step) for i, step in enumerate(steps)])
-        down(1, [later(lambda: None), later(relay, third[-2])])
+        down(1, turns[:-1])
     else:
         for p in third[2:]:
             arrive(p)
-        for p in third[:-1]:
+        for p in third[:-2]:
             relay(p)
-    down(0, [later(lambda: None), later(relay, third[-1])])
-    for p in third:
+    down(0, turns[:-1])
+    relay(third[-2])
+    if second:
+        for d in turns[:-1]:
+            pair_sum(1, d)
+        down(1, turns[-1:])
+    for d in turns[:-1]:
+        pair_sum(0, d)
+    relay(third[-1])
+    for p in third[:-1]:
         norm(p)
+    down(0, turns[-1:])
+    for g in range(last):
+        c2(g, 0).wait_recv()
+    norm(third[-1])
     steps = [later(send_back, p) for p in back[1]] if second else []
     hidden(third, [(2 * i + 1, step) for i, step in enumerate(steps)])
-    down(len(groups) - 1, [])
+    down(last, turns[:-1])
+    down_block(last, tp_of(y, oc))
+    c2(last, 0).start()
+    for d in turns[:-1]:
+        pair_sum(last, d)
+    down_block(last, t)
+    c2(last, 0).wait_recv()
     for p in back[0] + back[-1]:
         send_back(p)
 
@@ -663,6 +697,7 @@
             v((S * C, W), BF16),
             v((S * C, W), BF16),
             dma((12,)),
+            pltpu.SemaphoreType.REGULAR((max(1, (S - 1).bit_length()),)),
             dma((11,)),
             dma((2,)),
             dma((Y,)),

time: 58.5 us -> 56.4 us (0.964)
  Pallas kernels: 57.6 us -> 55.4 us
    pallas_call x1, Pallas kernels: 57.6 us -> 55.4 us  [per_device(): pl.pallas_call(functools.partial(kernel, S, T), out_shape=v((R, D), BF16)...]
where the time goes in v4:
time: 56.4 us; the launch traced here: 56.2 us
  Pallas kernels  55.4 us (98%)
  local copies, waits for them, and re-layouts  0.8 us (1%)
    pallas_call x1, Pallas kernels, per_device(): pl.pallas_call(functools.partial(kernel, S, T), out_shape=v((R, D), BF16)...  55.4 us

profile of v4, /device:TPU:0, one launch (start us, length us, event | category | flops | bytes accessed | tf_op | source)
XLA Modules:
  0.0 56.2 jit_solution(17691630408453701612)
XLA Ops:
  0.0 55.4 %layer.1 = bf16[128,2048]{1,0:T(8,128)(2,1)S(1)} custom-call(f32[1,8]{1,0:T(1,128)} %bitcast.7, bf16[128,512]{1,0:T(8,128)(2,1)} %q_hbm.1, bf16[128,256]{1,0:T(8,128)(2,1)} %k_hbm.1, bf16[128,256]{1,0:T(8,128)(2,1)} %v_hbm.1, bf16[128,2048]{1,0:T(8,128)(2,1)} %res_hbm.1, f32[1,2048]{1,0:T(1,128)} %bitcast.4, s32[2,128]{1,0:T(2,128)} %bitcast.5, ...), custom_call_target="tpu_custom_call" | custom-call | tf_op jit(solution)/shard_map/layer/pallas_call | solution.py:664
  55.4 0.8 %copy.14 = bf16[128,2048]{1,0:T(8,128)(2,1)} copy(bf16[128,2048]{1,0:T(8,128)(2,1)S(1)} %layer.1) | data formatting | bytes 1048576

commit v5 on v4

--- a/solution.py
+++ b/solution.py
@@ -89,7 +89,9 @@
     NH = y1_r.shape[1]
     HALO, C1, Y1, A, FY, FC, C2, Y2, B, GY, GC = (sent.at[i] for i in range(11))
     HW = W // NH
-    NF = gy_r.shape[1]
+    NF = a_r.shape[1]
+    NG = gy_r.shape[1]
+    GW = W // NG
     FW = W // NF
 
     me = lax.axis_index("sp")
@@ -403,6 +405,8 @@
         ).astype(BF16)
         for p in arrivals:
             a_send(p, j).start()
+    for f in range(NF):
+        a_fold(third[0], f).start()
     x_all[span(0), cols(t)] = picked[rows(me)]
 
     def forward(p, f):
@@ -488,8 +492,13 @@
             sb2[d - 1, at] = (
                 yp[at, cols(tp_of(yo(d), c))].astype(F32) + rc2[d, at].astype(F32)
             ).astype(BF16)
-            for f in range(NF):
-                y2_send(p, d, f).start()
+            if p:
+                for f in range(NF):
+                    y2_send(p, d, f).start()
+
+    def y2_own(d):
+        for f in range(NF):
+            y2_send(0, d, f).start()
 
     def down(g, turn):
         for d in turn:
@@ -524,11 +533,11 @@
         forward(0, f)
     for i, p in enumerate(arrivals):
         arrive(p)
-        if i == 0:
-            for q in third:
+        if i == 1:
+            for q in third[1:]:
                 for f in range(NF):
                     a_fold(q, f).start()
-        elif p <= split:
+        if 1 <= i and p <= split:
             relay(p - 2)
     for p in range(min(split, Z) - 1, split):
         relay(p)
@@ -545,7 +554,7 @@
         for p in second:
             norm(p)
         steps = [later(arrive, p) for p in third[2:]] + [later(relay, p) for p in third[:-2]]
-        hidden(second, [(i, step) for i, step in enumerate(steps)])
+        hidden(second, [(i + 1, step) for i, step in enumerate(steps)])
         down(1, turns[:-1])
     else:
         for p in third[2:]:
@@ -564,45 +573,57 @@
     for p in third[:-1]:
         norm(p)
     down(0, turns[-1:])
-    for g in range(last):
-        c2(g, 0).wait_recv()
+    if second:
+        c2(1, 0).wait_recv()
     norm(third[-1])
     steps = [later(send_back, p) for p in back[1]] if second else []
-    hidden(third, [(2 * i + 1, step) for i, step in enumerate(steps)])
+    hidden(third, [(NT - 2, step) for step in steps[:1]])
     down(last, turns[:-1])
+    for step in steps[1:]:
+        step()
     down_block(last, tp_of(y, oc))
     c2(last, 0).start()
     for d in turns[:-1]:
         pair_sum(last, d)
+        y2_own(d)
     down_block(last, t)
+    c2(0, 0).wait_recv()
+    for p in back[0][:-1]:
+        send_back(p)
     c2(last, 0).wait_recv()
-    for p in back[0] + back[-1]:
+    for p in back[-1] + [0]:
         send_back(p)
 
     others = pl.ds(0, (S - 1) * C)
     remote(rb.at[others], ret.at[others], B, b_r.at[0], sp=peer(1)).wait_recv()
 
+    def gwide(tt, j):
+        return pl.ds(pl.multiple_of(tt * W + j * GW, GW), GW)
+
+    def gfold(j):
+        return pl.ds(j * GW, GW)
+
     def gy_send(d, j):
-        ref = out.at[:, wide(t, j)]
+        ref = out.at[:, gwide(t, j)]
         return remote(ref, ref, GY, gy_r.at[seen(d), j], tp=tp_of(yo(d), c))
 
     def gy_recv(d, j):
-        ref = out.at[:, wide(tp_of(yo(d), c), j)]
+        ref = out.at[:, gwide(tp_of(yo(d), c), j)]
         return remote(ref, ref, GY, gy_r.at[d - 1, j], tp=tp_of(yo(d), c))
 
     def gc_send(d, j):
-        ref = out.at[:, wide(tp_of(yo(d), c), j)]
+        ref = out.at[:, gwide(tp_of(yo(d), c), j)]
         return remote(ref, ref, GC, gc_r.at[0], tp=tp_of(y, oc))
 
     pick0 = picker(slot0).astype(BF16)
     pick1 = picker(slot1).astype(BF16)
     rw0 = column(rw[0:1, :])
     rw1 = column(rw[1:2, :])
-    for j in range(NF):
-        mix0 = jnp.dot(pick0, ret[:, fold(j)], preferred_element_type=F32)
-        mix1 = jnp.dot(pick1, ret[:, fold(j)], preferred_element_type=F32)
-        out[:, wide(t, j)] = (
-            mixed[:, fold(j)].astype(F32) + (rw0 * mix0 + rw1 * mix1)
+    for j in range(NG):
+        mix0 = jnp.dot(pick0, ret[:, gfold(j)], preferred_element_type=F32)
+        mix1 = jnp.dot(pick1, ret[:, gfold(j)], preferred_element_type=F32)
+        out[:, gwide(t, j)] = (
+            mixed[:, gfold(j)].astype(F32) + (rw0 * mix0 + rw1 * mix1)
         ).astype(BF16)
         for d in range(1, Y):
             gy_send(d, j).start()
@@ -624,7 +645,7 @@
     drain(x_all.at[:, pl.ds(0, (Y - 1) * W)], Y2)
     drain(ret.at[others], B)
 
-    for j in range(NF):
+    for j in range(NG):
         for d in range(1, Y):
             gy_recv(d, j).wait_recv()
             gc_send(d, j).start()
@@ -657,7 +678,8 @@
     C = 2 * R * TOP // S
     FL = gate_weight.shape[2]
     NH = 4 if W % 512 == 0 else 1
-    NF = 2 if W % 256 == 0 else 1
+    NF = 4 if W % 512 == 0 else 1
+    NG = 2 if W % 256 == 0 else 1
     hbm = pl.BlockSpec(memory_space=pl.ANY)
     dma = pltpu.SemaphoreType.DMA
     v = pltpu.VMEM
@@ -708,7 +730,7 @@
             dma((3, Y)),
             dma((S, Y - 1, NF)),
             dma((1,)),
-            dma((Y - 1, NF)),
+            dma((Y - 1, NG)),
             dma((1,)),
         ],
         compiler_params=pltpu.CompilerParams(

time: 56.4 us -> 55.2 us (0.979)
  Pallas kernels: 55.4 us -> 54.3 us
    pallas_call x1, Pallas kernels: 55.4 us -> 54.3 us  [per_device(): pl.pallas_call(functools.partial(kernel, S, T), out_shape=v((R, D), BF16)...]
where the time goes in v5:
time: 55.2 us; the launch traced here: 55.1 us
  Pallas kernels  54.3 us (98%)
  local copies, waits for them, and re-layouts  0.8 us (1%)
    pallas_call x1, Pallas kernels, per_device(): pl.pallas_call(functools.partial(kernel, S, T), out_shape=v((R, D), BF16)...  54.3 us

profile of v5, /device:TPU:0, one launch (start us, length us, event | category | flops | bytes accessed | tf_op | source)
XLA Modules:
  0.0 55.1 jit_solution(9978806913523942729)
XLA Ops:
  0.0 54.3 %layer.1 = bf16[128,2048]{1,0:T(8,128)(2,1)S(1)} custom-call(f32[1,8]{1,0:T(1,128)} %bitcast.7, bf16[128,512]{1,0:T(8,128)(2,1)} %q_hbm.1, bf16[128,256]{1,0:T(8,128)(2,1)} %k_hbm.1, bf16[128,256]{1,0:T(8,128)(2,1)} %v_hbm.1, bf16[128,2048]{1,0:T(8,128)(2,1)} %res_hbm.1, f32[1,2048]{1,0:T(1,128)} %bitcast.4, s32[2,128]{1,0:T(2,128)} %bitcast.5, ...), custom_call_target="tpu_custom_call" | custom-call | tf_op jit(solution)/shard_map/layer/pallas_call | solution.py:686
  54.3 0.8 %copy.14 = bf16[128,2048]{1,0:T(8,128)(2,1)} copy(bf16[128,2048]{1,0:T(8,128)(2,1)S(1)} %layer.1) | data formatting | bytes 1048576

commit v6 on v5

--- a/solution.py
+++ b/solution.py
@@ -92,6 +92,8 @@
     NF = a_r.shape[1]
     NG = gy_r.shape[1]
     GW = W // NG
+    NB = y2_r.shape[2]
+    BW = W // NB
     FW = W // NF
 
     me = lax.axis_index("sp")
@@ -378,14 +380,14 @@
 
     def fy_send(p, d, f):
         ref = x_all.at[span(p), wide(t, f)]
-        return remote(ref, ref, FY, fy_r.at[p, seen(d), f], tp=tp_of(yo(d), c))
-
-    def fy_recv(p, d, f):
-        ref = x_all.at[span(p), wide(tp_of(yo(d), c), f)]
-        return remote(ref, ref, FY, fy_r.at[p, d - 1, f], tp=tp_of(yo(d), c))
-
-    def fc_send(p, d, f):
-        ref = x_all.at[span(p), wide(tp_of(yo(d), c), f)]
+        return remote(ref, ref, FY, fy_r.at[p, seen(d)], tp=tp_of(yo(d), c))
+
+    def fy_recv(p, d):
+        ref = x_all.at[span(p), cols(tp_of(yo(d), c))]
+        return remote(ref, ref, FY, fy_r.at[p, d - 1], tp=tp_of(yo(d), c))
+
+    def fc_send(p, d):
+        ref = x_all.at[span(p), cols(tp_of(yo(d), c))]
         return remote(ref, ref, FC, fc_r.at[p], tp=tp_of(y, oc))
 
     def fc_recv(p):
@@ -412,18 +414,17 @@
     def forward(p, f):
         for d in range(1, Y):
             fy_send(p, d, f).start()
-        fc_send(p, 0, f).start()
 
     def relay(p):
-        for f in range(NF):
-            for d in range(1, Y):
-                fy_recv(p, d, f).wait_recv()
-                fc_send(p, d, f).start()
+        for d in range(1, Y):
+            fy_recv(p, d).wait_recv()
+            fc_send(p, d).start()
 
     def arrive(p):
         for f in range(NF):
             a_fold(p, f).wait_recv()
             forward(p, f)
+        fc_send(p, 0).start()
 
     def norm(p):
         fc_recv(p).wait_recv()
@@ -464,10 +465,16 @@
             BF16
         )
 
+    def bwide(tt, f):
+        return pl.ds(pl.multiple_of(tt * W + f * BW, BW), BW)
+
+    def bfold(f):
+        return pl.ds(f * BW, BW)
+
     def y2_send(p, d, f):
         return remote(
-            sb2.at[d - 1, span(p), fold(f)],
-            ry2.at[seen(d), span(p), fold(f)],
+            sb2.at[d - 1, span(p), bfold(f)],
+            ry2.at[seen(d), span(p), bfold(f)],
             Y2,
             y2_r.at[p, seen(d), f],
             tp=tp_of(yo(d), c),
@@ -475,8 +482,8 @@
 
     def y2_recv(p, d, f):
         return remote(
-            sb2.at[d - 1, span(p), fold(f)],
-            ry2.at[d - 1, span(p), fold(f)],
+            sb2.at[d - 1, span(p), bfold(f)],
+            ry2.at[d - 1, span(p), bfold(f)],
             Y2,
             y2_r.at[p, d - 1, f],
             tp=tp_of(yo(d), c),
@@ -493,11 +500,11 @@
                 yp[at, cols(tp_of(yo(d), c))].astype(F32) + rc2[d, at].astype(F32)
             ).astype(BF16)
             if p:
-                for f in range(NF):
+                for f in range(NB):
                     y2_send(p, d, f).start()
 
     def y2_own(d):
-        for f in range(NF):
+        for f in range(NB):
             y2_send(0, d, f).start()
 
     def down(g, turn):
@@ -510,27 +517,28 @@
     def b_send(p, f):
         e = peer(p)
         return remote(
-            rb.at[span(p), fold(f)], ret.at[rows(me), fold(f)], B, b_r.at[0], sp=e
+            rb.at[span(p), bfold(f)], ret.at[rows(me), bfold(f)], B, b_r.at[0], sp=e
         )
 
     def send_back(p):
         at = span(p)
-        for f in range(NF):
-            total = yp[at, wide(t, f)].astype(F32) + rc2[0, at, fold(f)].astype(F32)
+        for f in range(NB):
+            total = yp[at, bwide(t, f)].astype(F32) + rc2[0, at, bfold(f)].astype(F32)
             for d in range(1, Y):
                 y2_recv(p, d, f).wait_recv()
-                total = total + ry2[d - 1, at, fold(f)].astype(F32)
+                total = total + ry2[d - 1, at, bfold(f)].astype(F32)
             if p:
-                rb[at, fold(f)] = total.astype(BF16)
+                rb[at, bfold(f)] = total.astype(BF16)
                 b_send(p, f).start()
             else:
-                ret[rows(me), fold(f)] = total.astype(BF16)
+                ret[rows(me), bfold(f)] = total.astype(BF16)
 
     def later(f, *args):
         return lambda: f(*args)
 
     for f in range(NF):
         forward(0, f)
+    fc_send(0, 0).start()
     for i, p in enumerate(arrivals):
         arrive(p)
         if i == 1:
@@ -678,8 +686,9 @@
     C = 2 * R * TOP // S
     FL = gate_weight.shape[2]
     NH = 4 if W % 512 == 0 else 1
-    NF = 4 if W % 512 == 0 else 1
+    NF = 2 if W % 256 == 0 else 1
     NG = 2 if W % 256 == 0 else 1
+    NB = 2 if W % 256 == 0 else 1
     hbm = pl.BlockSpec(memory_space=pl.ANY)
     dma = pltpu.SemaphoreType.DMA
     v = pltpu.VMEM
@@ -725,10 +734,10 @@
             dma((Y,)),
             dma((Y - 1, NH)),
             dma((S, NF)),
-            dma((S, Y - 1, NF)),
+            dma((S, Y - 1)),
             dma((S,)),
             dma((3, Y)),
-            dma((S, Y - 1, NF)),
+            dma((S, Y - 1, NB)),
             dma((1,)),
             dma((Y - 1, NG)),
             dma((1,)),

time: 55.2 us -> 54.5 us (0.987)
  Pallas kernels: 54.3 us -> 53.5 us
    pallas_call x1, Pallas kernels: 54.3 us -> 53.5 us  [per_device(): pl.pallas_call(functools.partial(kernel, S, T), out_shape=v((R, D), BF16)...]
where the time goes in v6:
time: 54.5 us; the launch traced here: 54.3 us
  Pallas kernels  53.5 us (98%)
  local copies, waits for them, and re-layouts  0.8 us (1%)
    pallas_call x1, Pallas kernels, per_device(): pl.pallas_call(functools.partial(kernel, S, T), out_shape=v((R, D), BF16)...  53.5 us

profile of v6, /device:TPU:0, one launch (start us, length us, event | category | flops | bytes accessed | tf_op | source)
XLA Modules:
  0.0 54.3 jit_solution(2407502452570558393)
XLA Ops:
  0.0 53.5 %layer.1 = bf16[128,2048]{1,0:T(8,128)(2,1)S(1)} custom-call(f32[1,8]{1,0:T(1,128)} %bitcast.7, bf16[128,512]{1,0:T(8,128)(2,1)} %q_hbm.1, bf16[128,256]{1,0:T(8,128)(2,1)} %k_hbm.1, bf16[128,256]{1,0:T(8,128)(2,1)} %v_hbm.1, bf16[128,2048]{1,0:T(8,128)(2,1)} %res_hbm.1, f32[1,2048]{1,0:T(1,128)} %bitcast.4, s32[2,128]{1,0:T(2,128)} %bitcast.5, ...), custom_call_target="tpu_custom_call" | custom-call | tf_op jit(solution)/shard_map/layer/pallas_call | solution.py:695
  53.5 0.8 %copy.14 = bf16[128,2048]{1,0:T(8,128)(2,1)} copy(bf16[128,2048]{1,0:T(8,128)(2,1)S(1)} %layer.1) | data formatting | bytes 1048576

commit v7 on v6

--- a/solution.py
+++ b/solution.py
@@ -204,7 +204,7 @@
             )
         )
     ]
-    for load in loads:
+    for load in loads[:8]:
         load.start()
     loads[0].wait()
     loads[1].wait()
@@ -221,6 +221,8 @@
             copy.start()
 
     meet(0)
+    for load in loads[8:]:
+        load.start()
     for load in loads[2:5]:
         load.wait()
 

time: 54.5 us -> 54.5 us (level)
  no operation moved by 1% of the time
where the time goes in v7:
time: 54.5 us; the launch traced here: 54.4 us
  Pallas kernels  53.5 us (98%)
  local copies, waits for them, and re-layouts  0.8 us (1%)
    pallas_call x1, Pallas kernels, per_device(): pl.pallas_call(functools.partial(kernel, S, T), out_shape=v((R, D), BF16)...  53.5 us

profile of v7, /device:TPU:0, one launch (start us, length us, event | category | flops | bytes accessed | tf_op | source)
XLA Modules:
  0.0 54.4 jit_solution(15584762248732246264)
XLA Ops:
  0.0 53.5 %layer.1 = bf16[128,2048]{1,0:T(8,128)(2,1)S(1)} custom-call(f32[1,8]{1,0:T(1,128)} %bitcast.7, bf16[128,512]{1,0:T(8,128)(2,1)} %q_hbm.1, bf16[128,256]{1,0:T(8,128)(2,1)} %k_hbm.1, bf16[128,256]{1,0:T(8,128)(2,1)} %v_hbm.1, bf16[128,2048]{1,0:T(8,128)(2,1)} %res_hbm.1, f32[1,2048]{1,0:T(1,128)} %bitcast.4, s32[2,128]{1,0:T(2,128)} %bitcast.5, ...), custom_call_target="tpu_custom_call" | custom-call | tf_op jit(solution)/shard_map/layer/pallas_call | solution.py:697
  53.6 0.8 %copy.14 = bf16[128,2048]{1,0:T(8,128)(2,1)} copy(bf16[128,2048]{1,0:T(8,128)(2,1)S(1)} %layer.1) | data formatting | bytes 1048576
